TPU v7x, 32 devices: a whole 2x2x4 slice. The times are simulated.
32 devices in a mesh: ep: 8 (over z, x), tp: 4 (over y, core).
Axes of the slice: x: 2, y: 2, z: 4, core: 2. Of those that a mesh axis runs over, the one named last changes fastest.
Arguments:
- mixer_input: bfloat16 [2048, 2048], P('ep', 'tp'), may hold values from -80 to 80
- mixer_gain: float32 [2048], P('tp'), may hold values from 0.1 to 1.9
- time_step: float32 [2048, 128], P('ep', 'tp'), may hold values from 0.25 to 4
- pole_real: float32 [128, 32], P('tp'), may hold values from -0.1 to 0, as said below
- pole_imag: float32 [128, 32], P('tp'), may hold values from 0.25 to 3
- input_real: float32 [128, 32, 16], P('tp'), may hold values from -1 to 1
- input_imag: float32 [128, 32, 16], P('tp'), may hold values from -1 to 1
- read_real: float32 [128, 16, 32], P('tp'), may hold values from -1 to 1
- read_imag: float32 [128, 16, 32], P('tp'), may hold values from -1 to 1
- out_value: bfloat16 [2048, 2048], P(None, 'tp'), may hold values from -0.125 to 0.125
- out_gate: bfloat16 [2048, 2048], P(None, 'tp'), may hold values from -0.125 to 0.125
- expert_input: bfloat16 [1024, 2048], P('ep', 'tp'), may hold values from -80 to 80
- expert_gain: float32 [2048], P('tp'), may hold values from 0.1 to 1.9
- routes: int32 [1024, 2], P('ep'), may hold values from 0 to 7, all different within a row; in each aligned block of 128 rows (0 to 127, 128 to 255, ...) at most 64 rows name the same one
- route_weight: float32 [1024, 2], P('ep'), may hold values from 0.2 to 1
- expert_gate: bfloat16 [8, 2048, 4096], P('ep', None, 'tp'), may hold values from -0.125 to 0.125
- expert_up: bfloat16 [8, 2048, 4096], P('ep', None, 'tp'), may hold values from -0.125 to 0.125
- expert_down: bfloat16 [8, 4096, 2048], P('ep', 'tp'), may hold values from -0.125 to 0.125
Outputs:
- mixer_output: bfloat16 [2048, 2048], P('ep', 'tp')
- expert_output: bfloat16 [1024, 2048], P('ep', 'tp')
Inputs may be any that keep to these rules, and one draw needn't show every extreme that they name: `routes`: each row names 2 different experts. Among the 128 rows of one index of ep, no expert is named more than 64 times, a bound that some block reaches in some of them. `pole_real`: every rate is negative.
All inputs are finite; a program needn't handle non-finite values.
Results may differ from a plain program's by a relative error of at most 0.02.
Values may be sent and summed in bfloat16 or wider, within the bound.
A program may use at most 128 MiB of HBM per device.

v0:
```python
import functools
import jax
import jax.numpy as jnp
from jax import lax
from jax.experimental import pallas as pl
from jax.experimental.pallas import tpu as pltpu
from jax.sharding import PartitionSpec as P

norm_eps = 1e-05
highest = lax.Precision.HIGHEST
CHUNKS = 8
TILE = 256


def sin_cos(angle):
    turns = jnp.round(angle * 0.6366197723675814)
    left = angle - turns * 1.5703125
    left = left - turns * 4.83751296997e-4
    left = left - turns * 7.549789948768648e-8
    sq = left * left
    sine = ((-1.9515295891e-4 * sq + 8.3321608736e-3) * sq - 1.6666654611e-1) * sq * left + left
    cosine = (
        ((2.443315711809948e-5 * sq - 1.388731625493765e-3) * sq + 4.166664568298827e-2) * sq * sq
        - 0.5 * sq
        + 1.0
    )
    quadrant = turns.astype(jnp.int32)
    odd = (quadrant & 1) == 1
    sin_out = jnp.where(odd, cosine, sine)
    cos_out = jnp.where(odd, sine, cosine)
    sin_out = jnp.where((quadrant & 2) == 2, -sin_out, sin_out)
    cos_out = jnp.where(((quadrant + 1) & 2) == 2, -cos_out, cos_out)
    return sin_out, cos_out


def nt(left, right, **kw):
    return lax.dot_general(
        left, right, (((1,), (1,)), ((), ())), preferred_element_type=jnp.float32, **kw
    )


def spread(table, row_div, lane_div):
    rows, width = table.shape
    lanes = width * (rows // row_div)
    src = lax.broadcasted_iota(jnp.int32, (width, lanes), 0)
    dst = lax.broadcasted_iota(jnp.int32, (width, lanes), 1)
    pick = (src == dst % width).astype(jnp.bfloat16)
    wide = jnp.dot(table.astype(jnp.bfloat16), pick, preferred_element_type=jnp.float32)
    row = lax.broadcasted_iota(jnp.int32, (rows, lanes), 0) // row_div
    lane = lax.broadcasted_iota(jnp.int32, (rows, lanes), 1) // lane_div
    return jnp.where(row == lane, wide, 0.0).astype(jnp.bfloat16)


def mixer_kernel(
    width,
    rows_ref,
    stats_ref,
    gain_ref,
    step_ref,
    pole_ref,
    in_re_ref,
    in_im_ref,
    rd_re_ref,
    rd_im_ref,
    out_ref,
    a_re,
    a_im,
    u_re,
    u_im,
    sums,
    enter,
    mixed_ref,
    mine_ref,
    slots_ref,
    send_sems,
    recv_sems,
):
    count = slots_ref.shape[0]
    me = lax.axis_index("ep")
    barrier = pltpu.get_barrier_semaphore()
    for k in range(1, count):
        pl.semaphore_signal(
            barrier,
            inc=1,
            device_id={"ep": lax.rem(me + k, count)},
            device_id_type=pl.DeviceIdType.MESH,
        )

    positions, channels = rows_ref.shape
    groups = step_ref.shape[1]
    flat = a_re.shape[1]
    states = flat // groups
    group_ch = channels // groups
    tiles = flat // TILE
    per_tile = TILE // states
    tile_ch = per_tile * group_ch
    steps = positions // CHUNKS

    average = stats_ref[:, 0:1] / width
    variance = stats_ref[:, 1:2] / width - average * average
    normed = (rows_ref[...].astype(jnp.float32) - average) * lax.rsqrt(variance + norm_eps)
    normed = (normed * gain_ref[...]).astype(jnp.bfloat16)
    to_row = lax.broadcasted_iota(jnp.int32, (positions, positions), 0)
    from_row = lax.broadcasted_iota(jnp.int32, (positions, positions), 1)
    order = from_row == (to_row % CHUNKS) * steps + to_row // CHUNKS
    order16 = order.astype(jnp.bfloat16)
    normed = jnp.dot(order16, normed, preferred_element_type=jnp.float32).astype(jnp.bfloat16)
    step = jnp.dot(
        order.astype(jnp.float32), step_ref[...], precision=highest,
        preferred_element_type=jnp.float32,
    )

    for tile in range(tiles):
        lanes = slice(tile * TILE, (tile + 1) * TILE)
        source = lax.broadcasted_iota(jnp.int32, (groups, TILE), 0)
        owner = lax.broadcasted_iota(jnp.int32, (groups, TILE), 1) // states + tile * per_tile
        a_re[:, lanes] = jnp.dot(
            step, (source == owner).astype(jnp.float32), precision=highest,
            preferred_element_type=jnp.float32,
        )
        piece = normed[:, tile * tile_ch : (tile + 1) * tile_ch]
        u_re[:, lanes] = nt(piece, spread(in_re_ref[lanes, :], states, group_ch))
        u_im[:, lanes] = nt(piece, spread(in_im_ref[lanes, :], states, group_ch))
        p_re, p_im = pole_ref[0:1, lanes], pole_ref[1:2, lanes]
        d_re, d_im = pole_ref[2:3, lanes], pole_ref[3:4, lanes]

        def first(s, carried, lanes=lanes, p_re=p_re, p_im=p_im, d_re=d_re, d_im=d_im):
            c_re, c_im, s_re, s_im = carried
            here = pl.ds(pl.multiple_of(s * CHUNKS, CHUNKS), CHUNKS)
            delta = a_re[here, lanes]
            magnitude = jnp.exp(p_re * delta)
            sine, cosine = sin_cos(p_im * delta)
            ab_re = magnitude * cosine
            ab_im = magnitude * sine
            numer = ab_re - 1.0
            k_re = numer * d_re + ab_im * d_im
            k_im = ab_im * d_re - numer * d_im
            v_re, v_im = u_re[here, lanes], u_im[here, lanes]
            w_re = k_re * v_re - k_im * v_im
            w_im = k_re * v_im + k_im * v_re
            a_re[here, lanes] = ab_re
            a_im[here, lanes] = ab_im
            u_re[here, lanes] = w_re
            u_im[here, lanes] = w_im
            return (
                ab_re * c_re - ab_im * c_im,
                ab_re * c_im + ab_im * c_re,
                ab_re * s_re - ab_im * s_im + w_re,
                ab_re * s_im + ab_im * s_re + w_im,
            )

        zero = jnp.zeros((CHUNKS, TILE), jnp.float32)
        found = lax.fori_loop(0, steps, first, (zero + 1.0, zero, zero, zero), unroll=4)
        for index, part in enumerate(found):
            sums[index, :, lanes] = part

    def chunk(index, c):
        return sums[index, c : c + 1, :]

    c_re, c_im, s_re, s_im = (chunk(index, 0) for index in range(4))
    for c in range(1, CHUNKS):
        b_re, b_im = chunk(0, c), chunk(1, c)
        c_re, c_im = b_re * c_re - b_im * c_im, b_re * c_im + b_im * c_re
        s_re, s_im = (
            b_re * s_re - b_im * s_im + chunk(2, c),
            b_re * s_im + b_im * s_re + chunk(3, c),
        )
    mine_ref[0:1, :] = c_re
    mine_ref[1:2, :] = c_im
    mine_ref[2:3, :] = s_re
    mine_ref[3:4, :] = s_im

    pl.semaphore_wait(barrier, count - 1)
    copies = []
    for k in range(1, count):
        copy = pltpu.make_async_remote_copy(
            src_ref=mine_ref,
            dst_ref=slots_ref.at[k],
            send_sem=send_sems.at[k],
            recv_sem=recv_sems.at[k],
            device_id={"ep": lax.rem(me + k, count)},
            device_id_type=pl.DeviceIdType.MESH,
        )
        copy.start()
        copies.append(copy)
    read_re = [
        spread(rd_re_ref[t * tile_ch : (t + 1) * tile_ch, :], group_ch, states)
        for t in range(tiles)
    ]
    read_im = [
        spread(rd_im_ref[t * tile_ch : (t + 1) * tile_ch, :], group_ch, states)
        for t in range(tiles)
    ]
    for copy in copies:
        copy.wait()

    def fold(position, carried):
        h_re, h_im = carried
        slot = me - position
        b_re, b_im = slots_ref[slot, 0:1, :], slots_ref[slot, 1:2, :]
        return (
            b_re * h_re - b_im * h_im + slots_ref[slot, 2:3, :],
            b_re * h_im + b_im * h_re + slots_ref[slot, 3:4, :],
        )

    blank = jnp.zeros((1, flat), jnp.float32)
    h_re, h_im = lax.fori_loop(0, me, fold, (blank, blank))
    for c in range(CHUNKS):
        enter[0, c : c + 1, :] = h_re
        enter[1, c : c + 1, :] = h_im
        b_re, b_im = chunk(0, c), chunk(1, c)
        h_re, h_im = (
            b_re * h_re - b_im * h_im + chunk(2, c),
            b_re * h_im + b_im * h_re + chunk(3, c),
        )

    for tile in range(tiles):
        lanes = slice(tile * TILE, (tile + 1) * TILE)

        def second(s, carried, lanes=lanes):
            s_re, s_im = carried
            here = pl.ds(pl.multiple_of(s * CHUNKS, CHUNKS), CHUNKS)
            ab_re, ab_im = a_re[here, lanes], a_im[here, lanes]
            n_re = ab_re * s_re - ab_im * s_im + u_re[here, lanes]
            n_im = ab_re * s_im + ab_im * s_re + u_im[here, lanes]
            u_re[here, lanes] = n_re
            u_im[here, lanes] = n_im
            return n_re, n_im

        lax.fori_loop(0, steps, second, (enter[0, :, lanes], enter[1, :, lanes]), unroll=8)
        response = nt(u_re[:, lanes].astype(jnp.bfloat16), read_re[tile]) - nt(
            u_im[:, lanes].astype(jnp.bfloat16), read_im[tile]
        )
        mixed_ref[:, tile * tile_ch : (tile + 1) * tile_ch] = jax.nn.gelu(response).astype(
            jnp.bfloat16
        )
    back = (to_row == (from_row % CHUNKS) * steps + from_row // CHUNKS).astype(jnp.bfloat16)
    out_ref[...] = jnp.dot(
        back, mixed_ref[...], preferred_element_type=jnp.float32
    ).astype(jnp.bfloat16)


def mix(rows, stats, gain, step, pole, in_re, in_im, rd_re, rd_im, width):
    positions, channels = rows.shape
    flat = pole.shape[1]
    count = lax.axis_size("ep")
    f32 = jnp.float32
    return pl.pallas_call(
        functools.partial(mixer_kernel, width),
        out_shape=jax.ShapeDtypeStruct((positions, channels), jnp.bfloat16),
        in_specs=[pl.BlockSpec(memory_space=pltpu.VMEM)] * 9,
        out_specs=pl.BlockSpec(memory_space=pltpu.VMEM),
        scratch_shapes=[
            pltpu.VMEM((positions, flat), f32),
            pltpu.VMEM((positions, flat), f32),
            pltpu.VMEM((positions, flat), f32),
            pltpu.VMEM((positions, flat), f32),
            pltpu.VMEM((4, CHUNKS, flat), f32),
            pltpu.VMEM((2, CHUNKS, flat), f32),
            pltpu.VMEM((positions, channels), jnp.bfloat16),
            pltpu.VMEM((4, flat), f32),
            pltpu.VMEM((count, 4, flat), f32),
            pltpu.SemaphoreType.DMA((count,)),
            pltpu.SemaphoreType.DMA((count,)),
        ],
        compiler_params=pltpu.CompilerParams(
            collective_id=0, has_side_effects=True, vmem_limit_bytes=24 * 1024 * 1024
        ),
        cost_estimate=pl.CostEstimate(
            flops=2 * positions * flat * 400, bytes_accessed=4 * positions * flat, transcendentals=0
        ),
    )(rows, stats, gain, step, pole, in_re, in_im, rd_re, rd_im)


def moments_kernel(a_ref, b_ref, out_a_ref, out_b_ref, mine_ref, slots_ref, send_sems, recv_sems):
    count = slots_ref.shape[0]
    me = lax.axis_index("tp")
    barrier = pltpu.get_barrier_semaphore()
    for k in range(1, count):
        pl.semaphore_signal(
            barrier,
            inc=1,
            device_id={"tp": lax.rem(me + k, count)},
            device_id_type=pl.DeviceIdType.MESH,
        )
    split = a_ref.shape[0]
    ones = jnp.ones((8, a_ref.shape[1]), jnp.float32)
    first = lax.broadcasted_iota(jnp.int32, (8, 1), 0) == 0
    for rows_ref, lanes in ((a_ref, slice(0, split)), (b_ref, slice(split, None))):
        wide = rows_ref[...].astype(jnp.float32)
        sums = nt(ones, wide, precision=highest)
        squares = nt(ones, wide * wide, precision=highest)
        mine_ref[:, lanes] = jnp.where(first, sums, squares)
    pl.semaphore_wait(barrier, count - 1)
    copies = []
    for k in range(1, count):
        copy = pltpu.make_async_remote_copy(
            src_ref=mine_ref,
            dst_ref=slots_ref.at[k],
            send_sem=send_sems.at[k],
            recv_sem=recv_sems.at[k],
            device_id={"tp": lax.rem(me + k, count)},
            device_id_type=pl.DeviceIdType.MESH,
        )
        copy.start()
        copies.append(copy)
    total = mine_ref[...]
    for k, copy in enumerate(copies):
        copy.wait()
        total = total + slots_ref[k + 1]
    turned = total.T
    out_a_ref[...] = turned[:split, :]
    out_b_ref[...] = turned[split:, :]


def moments(rows_a, rows_b):
    count = lax.axis_size("tp")
    size = rows_a.shape[0] + rows_b.shape[0]
    f32 = jnp.float32
    return pl.pallas_call(
        moments_kernel,
        out_shape=[
            jax.ShapeDtypeStruct((rows_a.shape[0], 8), f32),
            jax.ShapeDtypeStruct((rows_b.shape[0], 8), f32),
        ],
        in_specs=[pl.BlockSpec(memory_space=pltpu.VMEM)] * 2,
        out_specs=[pl.BlockSpec(memory_space=pltpu.VMEM)] * 2,
        scratch_shapes=[
            pltpu.VMEM((8, size), f32),
            pltpu.VMEM((count, 8, size), f32),
            pltpu.SemaphoreType.DMA((count,)),
            pltpu.SemaphoreType.DMA((count,)),
        ],
        compiler_params=pltpu.CompilerParams(
            collective_id=1, has_side_effects=True, vmem_limit_bytes=16 * 1024 * 1024
        ),
    )(rows_a, rows_b)


def normalize(rows, sums, squares, gain, width):
    average = sums / width
    variance = squares / width - average * average
    wide = rows.astype(jnp.float32)
    return (wide - average[:, None]) * lax.rsqrt(variance[:, None] + norm_eps) * gain[None, :]


def shards(
    mixer_input,
    mixer_gain,
    time_step,
    pole_real,
    pole_imag,
    input_real,
    input_imag,
    read_real,
    read_imag,
    out_value,
    out_gate,
    expert_input,
    expert_gain,
    routes,
    route_weight,
    expert_gate,
    expert_up,
    expert_down,
):
    width = mixer_input.shape[1] * lax.axis_size("tp")
    stats_a, stats_b = moments(mixer_input, expert_input)
    sums_b, squares_b = stats_b[:, 0], stats_b[:, 1]
    normed_b = normalize(expert_input, sums_b, squares_b, expert_gain, width).astype(jnp.bfloat16)
    tokens_dev, top_count = routes.shape
    expert_count = lax.axis_size("ep")
    capacity = 2 * top_count * tokens_dev // expert_count
    flat_routes = routes.reshape(-1)
    onehot = (flat_routes[:, None] == jnp.arange(expert_count, dtype=jnp.int32)[None, :]).astype(
        jnp.int32
    )
    earlier_hits = jnp.cumsum(onehot, axis=0) - onehot
    position = jnp.sum(earlier_hits * onehot, axis=1)
    slot_index = (flat_routes * capacity + position).reshape(tokens_dev, top_count)
    slots = jnp.arange(expert_count * capacity, dtype=jnp.int32)
    named = slot_index[:, :, None] == slots[None, None, :]
    gate_weight = expert_gate[0]
    up_weight = expert_up[0]
    down_weight = expert_down[0]
    chosen = jnp.any(named, axis=1).astype(jnp.bfloat16)
    outgoing = lax.dot_general(
        chosen, normed_b, (((0,), (0,)), ((), ())), preferred_element_type=jnp.float32
    ).astype(jnp.bfloat16)
    arrived = lax.all_to_all(outgoing, "ep", split_axis=0, concat_axis=0, tiled=True)
    flat_real = pole_real.reshape(-1)
    flat_imag = pole_imag.reshape(-1)
    denom = flat_real * flat_real + flat_imag * flat_imag
    pole = jnp.stack([flat_real, flat_imag, flat_real / denom, flat_imag / denom])
    arrived, stats_a = lax.optimization_barrier((arrived, stats_a))
    arrived = lax.all_gather(arrived, "tp", axis=1, tiled=True)
    mixed = mix(
        mixer_input,
        stats_a,
        mixer_gain[None, :],
        time_step,
        pole,
        input_real.reshape(-1, input_real.shape[2]),
        input_imag.reshape(-1, input_imag.shape[2]),
        read_real.reshape(-1, read_real.shape[2]),
        read_imag.reshape(-1, read_imag.shape[2]),
        width,
    )
    arrived, mixed = lax.optimization_barrier((arrived, mixed))
    piece = lax.all_gather(mixed, "tp", axis=1, tiled=True)
    gate_val = jnp.dot(arrived, gate_weight, preferred_element_type=jnp.float32)
    up_val = jnp.dot(arrived, up_weight, preferred_element_type=jnp.float32)
    hidden = (jax.nn.silu(gate_val) * up_val).astype(jnp.bfloat16)
    summed = lax.psum_scatter(
        lax.dot_general(
            down_weight, hidden, (((0,), (1,)), ((), ())), preferred_element_type=jnp.float32
        ).astype(jnp.bfloat16),
        "tp",
        scatter_dimension=0,
        tiled=True,
    )
    value_sum = jnp.dot(piece, out_value, preferred_element_type=jnp.float32)
    gate_sum = jnp.dot(piece, out_gate, preferred_element_type=jnp.float32)
    mixer_output = (value_sum * jax.nn.sigmoid(gate_sum)).astype(jnp.bfloat16)
    returned = lax.all_to_all(summed, "ep", split_axis=1, concat_axis=1, tiled=True)
    share = jnp.sum(jnp.where(named, route_weight[:, :, None], 0.0), axis=1)
    share_high = share.astype(jnp.bfloat16)
    share_low = (share - share_high.astype(jnp.float32)).astype(jnp.bfloat16)
    expert_output = (nt(share_high, returned) + nt(share_low, returned)).astype(jnp.bfloat16)
    return (mixer_output, expert_output)


def solution(mesh):
    return jax.shard_map(
        shards,
        mesh=mesh,
        in_specs=(
            P("ep", "tp"),
            P("tp"),
            P("ep", "tp"),
            P("tp", None),
            P("tp", None),
            P("tp", None, None),
            P("tp", None, None),
            P("tp", None, None),
            P("tp", None, None),
            P(None, "tp"),
            P(None, "tp"),
            P("ep", "tp"),
            P("tp"),
            P("ep", None),
            P("ep", None),
            P("ep", None, "tp"),
            P("ep", None, "tp"),
            P("ep", "tp", None),
        ),
        out_specs=(P("ep", "tp"), P("ep", "tp")),
        check_vma=False,
    )
```

profile of v0, /device:TPU:0, one launch (start us, length us, event | category | flops | bytes accessed | tf_op | source)
XLA Modules:
  0.0 139.3 jit_solution(16979764318124036610)
XLA Ops:
  7.3 0.9 copy.41
  8.5 0.6 reduce-window.6
  9.6 0.7 multiply_add_fusion.1
  10.5 0.9 copy-done.1
  11.4 0.9 copy-done.3
  12.3 6.2 %shard_map.185 = (f32[256,8]{1,0:T(8,128)S(1)}, f32[128,8]{1,0:T(8,128)S(1)}) custom-call(bf16[256,512]{1,0:T(8,128)(2,1)S(1)} %copy-done.1, bf16[128,512]{1,0:T(8,128)(2,1)S(1)} %copy-done.3), custom_call_target="tpu_custom_call" | custom-call | tf_op jit(solution)/shard_map/pallas_call | solution.py:320
  18.8 1.1 convolution_convert_fusion
  19.9 20.5 %all_to_all.24 = bf16[8,64,512]{2,1,0:T(8,128)(2,1)} all-to-all(bf16[8,64,512]{2,1,0:T(8,128)(2,1)S(1)} %bitcast.53), channel_id=1, replica_groups=mesh['ep'=8,'tp'=4] {'ep'}, dimensions={0} | all-to-all | bytes 1048576 | tf_op jit(solution)/shard_map/all_to_all | solution.py:390
  41.0 1.2 copy.45
  42.2 0.9 copy-done.4
  43.2 0.9 copy-done.5
  44.1 0.9 copy-done.7
  45.0 13.5 %shard_map.186 = bf16[256,512]{1,0:T(8,128)(2,1)} custom-call(bf16[256,512]{1,0:T(8,128)(2,1)S(1)} %copy-done.2, f32[256,8]{1,0:T(8,128)S(1)} %copy-done.7, f32[1,512]{1,0:T(1,128)S(1)} %bitcast.49, f32[256,32]{1,0:T(8,128)S(1)} %copy.46.step_ref, f32[4,1024]{1,0:T(4,128)S(1)} %pad_maximum_fusion.pole_ref, f32[1024,16]{1,0:T(8,128)S(1)} %bitcast.45, ...), custom_call_target="tpu_custom_call" | custom-call | flops 209715200 | bytes 1048576 | tf_op jit(solution)/shard_map/pallas_call | solution.py:248
  58.5 2.8 %all-gather.3.cloned.1.call-done = bf16[512,2048]{1,0:T(8,128)(2,1)} async-done(((bf16[512,512]{1,0:T(8,128)(2,1)}), bf16[512,2048]{1,0:T(8,128)(2,1)}) %all-gather.3.cloned.1.call-update) | async-done | bytes 2097168 | tf_op jit(solution)/shard_map/all_gather | solution.py:396
  61.4 6.5 %fusion.4 = f32[512,1024]{1,0:T(8,128)} fusion(bf16[512,2048]{1,0:T(8,128)(2,1)} %all-gather.3.cloned.1.call-done, bf16[1,2048,1024]{2,1,0:T(8,128)(2,1)} %param.33), kind=kOutput, calls=%fused_computation.4 | convolution fusion | flops 2147483648 | bytes 8388608 | tf_op jit(solution)/shard_map/dot_general | solution.py:411
  67.8 10.5 %fusion.9 = bf16[2048,512]{0,1:T(8,128)(2,1)} fusion(bf16[1,1024,2048]{2,1,0:T(8,128)(2,1)} %param.35, f32[512,1024]{1,0:T(8,128)} %fusion.4, bf16[512,2048]{1,0:T(8,128)(2,1)} %all-gather.3.cloned.1.call-done, bf16[1,2048,1024]{2,1,0:T(8,128)(2,1)} %param.34), kind=kOutput, calls=%fused_computation.7 | convolution fusion | flops 4299161600 | bytes 14680064 | tf_op jit(solution)/shard_map/dot_general | solution.py:415
  78.5 0.7 all-gather.5.cloned.1.call-update
  79.1 30.6 %reduce-scatter.2.cloned.1.call-done = bf16[512,512]{0,1:T(8,128)(2,1)} async-done(((bf16[2048,512]{0,1:T(8,128)(2,1)}), bf16[512,512]{0,1:T(8,128)(2,1)}) %reduce-scatter.2.cloned.1.call-update) | async-done | bytes 524304 | tf_op jit(solution)/shard_map/reduce_scatter | solution.py:414
  109.7 5.5 %all-to-all-start.1 = ((bf16[512,8,64]{0,2,1:T(8,128)(2,1)}), bf16[512,8,64]{0,2,1:T(8,128)(2,1)S(1)}, u32[]{:S(2)}, u32[]{:S(2)}) async-start(bf16[512,8,64]{0,2,1:T(8,128)(2,1)} %bitcast.54), calls=%async_computation.2 | async-start | bytes 1048576 | tf_op jit(solution)/shard_map/all_to_all | solution.py:425
  115.4 12.6 %all-gather.5.cloned.1.call-done = bf16[256,2048]{1,0:T(8,128)(2,1)} async-done(((bf16[256,512]{1,0:T(8,128)(2,1)}), bf16[256,2048]{1,0:T(8,128)(2,1)}) %all-gather.5.cloned.1.call-update) | async-done | bytes 1048592 | tf_op jit(solution)/shard_map/all_gather | solution.py:410
  128.1 2.2 %fusion.16 = f32[256,512]{1,0:T(8,128)S(1)} fusion(bf16[256,2048]{1,0:T(8,128)(2,1)} %all-gather.5.cloned.1.call-done, bf16[2048,512]{1,0:T(8,128)(2,1)S(1)} %copy-done), kind=kOutput, calls=%fused_computation.14 | convolution fusion | flops 537264128 | bytes 3670016 | tf_op jit(solution)/shard_map/dot_general | solution.py:423
  130.2 1.4 %fusion.17 = bf16[256,512]{1,0:T(8,128)(2,1)} fusion(f32[256,512]{1,0:T(8,128)S(1)} %fusion.16, bf16[256,2048]{1,0:T(8,128)(2,1)S(1)} %copy-done.10, bf16[2048,512]{1,0:T(8,128)(2,1)S(1)} %copy-done.9), kind=kOutput, calls=%fused_computation.15 | convolution fusion | flops 537133056 | bytes 3932160 | tf_op jit(solution)/shard_map/dot_general | solution.py:422
  131.7 0.2 fusion.26
  131.9 0.9 fusion.18
  (51 shorter events, 2.0 us)
Async XLA Ops:
  7.2 120.9 %copy-start = (bf16[2048,512]{1,0:T(8,128)(2,1)S(1)}, bf16[2048,512]{1,0:T(8,128)(2,1)}, u32[]{:S(2)}) copy-start(bf16[2048,512]{1,0:T(8,128)(2,1)} %param.28) | copy-start | bytes 6291460
  7.2 33.3 %copy-start.12 = (f32[256,32]{0,1:T(8,128)S(1)}, f32[256,32]{0,1:T(8,128)}, u32[]{:S(2)}) copy-start(f32[256,32]{0,1:T(8,128)} %param.20) | copy-start | bytes 98308
  7.2 33.4 %copy-start.13 = (f32[32,32]{1,0:T(8,128)S(1)}, f32[32,32]{1,0:T(8,128)}, u32[]{:S(2)}) copy-start(f32[32,32]{1,0:T(8,128)} %param.21) | copy-start | bytes 12292
  7.2 33.5 %copy-start.14 = (f32[32,32]{1,0:T(8,128)S(1)}, f32[32,32]{1,0:T(8,128)}, u32[]{:S(2)}) copy-start(f32[32,32]{1,0:T(8,128)} %param.22) | copy-start | bytes 12292
  7.2 33.5 %copy-start.11 = (f32[32,32,16]{1,2,0:T(8,128)S(1)}, f32[32,32,16]{1,2,0:T(8,128)}, u32[]{:S(2)}) copy-start(f32[32,32,16]{1,2,0:T(8,128)} %param.23) | copy-start | bytes 196612
  7.2 54.2 %all-gather.3.cloned.1.call-start = ((), (), s32[]{:S(2)}) async-start(), calls=%async_computation.3 | async-start | bytes 2621440 | tf_op jit(solution)/shard_map/all_gather | solution.py:396
  10.5 1.0 copy-start.1
  11.4 0.9 copy-start.3
  18.6 1.4 copy-start.6
  18.7 23.4 %copy-start.2 = (bf16[256,512]{1,0:T(8,128)(2,1)S(1)}, bf16[256,512]{1,0:T(8,128)(2,1)}, u32[]{:S(2)}) copy-start(bf16[256,512]{1,0:T(8,128)(2,1)} %rows_ref.1) | copy-start | bytes 786436
  18.8 23.4 %copy-start.8 = (f32[512]{0:T(512)S(1)}, f32[512]{0:T(512)}, u32[]{:S(2)}) copy-start(f32[512]{0:T(512)} %param.19) | copy-start | bytes 6148
  40.4 69.3 %reduce-scatter.2.cloned.1.call-start = ((), (), s32[]{:S(2)}) async-start(), calls=%async_computation.5 | async-start | bytes 2621440 | tf_op jit(solution)/shard_map/reduce_scatter | solution.py:414
  42.2 1.0 copy-start.4
  43.2 0.9 copy-start.5
  44.1 0.9 copy-start.7
  78.4 36.9 %copy-start.15 = (f32[128,2]{0,1:T(2,128)S(1)}, f32[128,2]{0,1:T(2,128)}, u32[]{:S(2)}) copy-start(f32[128,2]{0,1:T(2,128)} %param.32) | copy-start | bytes 3076
  78.4 49.6 %all-gather.5.cloned.1.call-start = ((), (), s32[]{:S(2)}) async-start(), calls=%async_computation.4 | async-start | bytes 1310720 | tf_op jit(solution)/shard_map/all_gather | solution.py:410
  109.7 21.9 %all-to-all-start.1 = ((bf16[512,8,64]{0,2,1:T(8,128)(2,1)}), bf16[512,8,64]{0,2,1:T(8,128)(2,1)S(1)}, u32[]{:S(2)}, u32[]{:S(2)}) async-start(bf16[512,8,64]{0,2,1:T(8,128)(2,1)} %bitcast.54), calls=%async_computation.2 | async-start | bytes 1048576 | tf_op jit(solution)/shard_map/all_to_all | solution.py:425
  128.0 2.2 %copy-start.9 = (bf16[2048,512]{1,0:T(8,128)(2,1)S(1)}, bf16[2048,512]{1,0:T(8,128)(2,1)}, u32[]{:S(2)}) copy-start(bf16[2048,512]{1,0:T(8,128)(2,1)} %param.27) | copy-start | bytes 6291460
  128.1 2.2 %copy-start.10 = (bf16[256,2048]{1,0:T(8,128)(2,1)S(1)}, bf16[256,2048]{1,0:T(8,128)(2,1)}, u32[]{:S(2)}) copy-start(bf16[256,2048]{1,0:T(8,128)(2,1)} %all-gather.5.cloned.1.call-done) | copy-start | bytes 3145732
Sparse Core Ops, SparseCore 0:
  40.5 20.7 all-gather.2
  78.5 31.1 reduce-scatter.1
  111.3 16.6 all-gather.4
where the time goes:
time: 140 us; the launch traced here: 139 us
  waiting for transfers between devices  46.8 us (33%)
  matrix products  22.8 us (16%)
  blocking collectives  20.5 us (15%)
  Pallas kernels  19.7 us (14%)
  between operations  14 us (10%)
  local copies, waits for them, and re-layouts  8 us (6%)
  starting transfers between devices  5.63 us (4%)
  other arithmetic  1.89 us (1%)
    reduce_scatter x1, waiting for transfers between devices, shards(): lax.psum_scatter(lax.dot_general(down_weight, hidden, (((0,), (1,)), ((),...  30.6 us
    all_to_all x1, blocking collectives, shards(): lax.all_to_all(outgoing, 'ep', split_axis=0, concat_axis=0, tiled=True)  20.5 us
    pallas_call x1, Pallas kernels, mix(): pl.pallas_call(functools.partial(mixer_kernel, width), out_shape=jax.Shap...  13.5 us
    all_gather x1, waiting for transfers between devices, shards(): piece = lax.all_gather(mixed, 'tp', axis=1, tiled=True)  12.6 us
    dot_general x1, matrix products, shards(): lax.dot_general(down_weight, hidden, (((0,), (1,)), ((), ())), preferred_...  10.5 us
    unnamed x36, local copies, waits for them, and re-layouts  7.14 us
    dot_general x1, matrix products, shards(): gate_val = jnp.dot(arrived, gate_weight, preferred_element_type=jnp.float32)  6.46 us
    pallas_call x1, Pallas kernels, moments(): pl.pallas_call(moments_kernel, out_shape=[jax.ShapeDtypeStruct((rows_a.sh...  6.22 us
  transfers between devices with their start and end apart: 4, of which 3 were waited for; matrix products, arithmetic and copies ran while one was open for 4% of the time, Pallas kernels for 10%

commit v1 on v0

v1 whole, which is shorter than its diff:
```python
import functools
import jax
import jax.numpy as jnp
from jax import lax
from jax.experimental import pallas as pl
from jax.experimental.pallas import tpu as pltpu
from jax.sharding import PartitionSpec as P

norm_eps = 1e-05
CHUNKS = 8
CORES = 2
f32 = jnp.float32
bf16 = jnp.bfloat16


def sin_cos(angle):
    turns = jnp.round(angle * 0.6366197723675814)
    left = angle - turns * 1.5703125
    left = left - turns * 4.83751296997e-4
    left = left - turns * 7.549789948768648e-8
    sq = left * left
    sine = ((-1.9515295891e-4 * sq + 8.3321608736e-3) * sq - 1.6666654611e-1) * sq * left + left
    cosine = (
        ((2.443315711809948e-5 * sq - 1.388731625493765e-3) * sq + 4.166664568298827e-2) * sq * sq
        - 0.5 * sq
        + 1.0
    )
    quadrant = turns.astype(jnp.int32)
    odd = (quadrant & 1) == 1
    sin_out = jnp.where(odd, cosine, sine)
    cos_out = jnp.where(odd, sine, cosine)
    sin_out = jnp.where((quadrant & 2) == 2, -sin_out, sin_out)
    cos_out = jnp.where(((quadrant + 1) & 2) == 2, -cos_out, cos_out)
    return sin_out, cos_out


def iota(shape, dim):
    return lax.broadcasted_iota(jnp.int32, shape, dim)


def nn(left, right):
    return jnp.dot(left, right, preferred_element_type=f32)


def nt(left, right):
    return lax.dot_general(left, right, (((1,), (1,)), ((), ())), preferred_element_type=f32)


def tn(left, right):
    return lax.dot_general(left, right, (((0,), (0,)), ((), ())), preferred_element_type=f32)


def partner(me, k):
    other, bit = me, 1
    while bit <= k:
        if k & bit:
            other = other + bit * (1 - 2 * ((me // bit) % 2))
        bit *= 2
    return other


def spread(table, row_div, lanes, lane_div):
    rows, width = table.shape
    pick = (iota((width, lanes), 0) == iota((width, lanes), 1) % width).astype(bf16)
    wide = nn(table.astype(bf16), pick)
    same = iota((rows, lanes), 0) // row_div == iota((rows, lanes), 1) // lane_div
    return jnp.where(same, wide, 0.0).astype(bf16)


def row_sums(rows):
    ones = jnp.ones((16, rows.shape[1]), bf16)
    wide = rows.astype(f32)
    square = wide * wide
    high = square.astype(bf16)
    low = (square - high.astype(f32)).astype(bf16)
    sums = nt(ones, rows)
    squares = nt(ones, high) + nt(ones, low)
    return jnp.where(iota((8, 1), 0) == 0, sums[:8], squares[:8])


def normalize(rows, stats, gain, width):
    average = stats[:, 0:1] / width
    variance = stats[:, 1:2] / width - average * average
    return (rows.astype(f32) - average) * lax.rsqrt(variance + norm_eps) * gain


def kernel(dims, *refs):
    count_ep, count_tp, groups_y, halves, state_size = dims
    hbm, refs = refs[:17], refs[17:]
    (out_a, out_b), refs = refs[:2], refs[2:]
    vm, refs = refs[:17], refs[17:]
    (
        mine_stats, slot_stats, outgoing, rows_x, share_hi, share_lo, a_re, a_im, u_re, u_im,
        sums, enter, mine_state, slot_state, n_re, n_im, mixed, mixed_all, hidden, own,
        sib_send, sib_recv, y_send, y_recv, final, returned,
        sem_in, st_s, st_r, aa_s, aa_r, dy_s, dy_r, ds_s, ds_r, hs_s, hs_r,
        my_s, my_r, ms_s, ms_r, rs_s, rs_r, ry_s, ry_r, ra_s, ra_r,
    ) = refs
    (
        a_in, step_in, gain_a, pole_in, in_re, in_im, rd_re, rd_im, w_value, w_gate_out,
        b_in, gain_b, routes_in, weight_in, w_gate, w_up, w_down,
    ) = vm

    me = lax.axis_index("ep")
    tp = lax.axis_index("tp")
    count_y = count_tp // CORES
    my_y = tp // CORES
    my_core = tp % CORES
    sibling = my_y * CORES + 1 - my_core

    barrier = pltpu.get_barrier_semaphore()
    for k in range(1, count_ep):
        pl.semaphore_signal(
            barrier, inc=1, device_id={"ep": partner(me, k)}, device_id_type=pl.DeviceIdType.MESH
        )
    for k in range(1, count_tp):
        pl.semaphore_signal(
            barrier, inc=1, device_id={"tp": lax.rem(tp + k, count_tp)},
            device_id_type=pl.DeviceIdType.MESH,
        )

    loads = [
        pltpu.make_async_copy(source, target, sem_in.at[i])
        for i, (source, target) in enumerate(zip(hbm, vm))
    ]
    for i in (10, 0, 12, 13, 11, 1, 3, 2, 4, 5, 6, 7, 14, 15, 16, 8, 9):
        loads[i].start()

    pending = []

    def send(source, target, send_sem, recv_sem, **where):
        copy = pltpu.make_async_remote_copy(
            src_ref=source, dst_ref=target, send_sem=send_sem, recv_sem=recv_sem,
            device_id=where, device_id_type=pl.DeviceIdType.MESH,
        )
        copy.start()
        pending.append(copy)
        return copy

    positions, channels = a_in.shape
    tokens, feats = b_in.shape
    width = feats * count_tp
    flat = a_re.shape[1]
    states = state_size
    group_ch = in_re.shape[0] * states // flat
    slots = rows_x.shape[0]
    cap = slots // count_ep
    tile = min(256, flat)
    tiles = flat // tile
    tile_ch = tile // states * group_ch
    steps = positions // CHUNKS
    hid = w_gate.shape[1]
    expert_rows = max(16, count_ep)
    my_cols = pl.ds(pl.multiple_of(tp * feats, 128), feats)

    loads[10].wait()
    loads[0].wait()
    mine_stats[:, :tokens] = row_sums(b_in[...])
    mine_stats[:, tokens:] = row_sums(a_in[...])
    pl.semaphore_wait(barrier, count_ep + count_tp - 2)
    stat_copies = [
        send(mine_stats, slot_stats.at[k], st_s.at[k], st_r.at[k], tp=lax.rem(tp + k, count_tp))
        for k in range(1, count_tp)
    ]

    loads[12].wait()
    loads[13].wait()
    expert_of = iota((expert_rows, tokens), 0)
    hit = jnp.zeros((expert_rows, tokens), jnp.bool_)
    weight = jnp.zeros((expert_rows, tokens), f32)
    for k in range(routes_in.shape[0]):
        this = routes_in[k : k + 1, :] == expert_of
        hit = jnp.logical_or(hit, this)
        weight = jnp.where(this, weight_in[k : k + 1, :], weight)
    before = (iota((tokens, tokens), 0) < iota((tokens, tokens), 1)).astype(bf16)
    place = nn(hit.astype(f32).astype(bf16), before)
    place = jnp.where(hit, place, -1.0).astype(bf16)
    owner = jnp.concatenate(
        [
            (iota((cap, expert_rows), 1) == partner(me, k)).astype(f32)
            for k in range(count_ep)
        ],
        axis=0,
    ).astype(bf16)
    chosen = nn(owner, place) == (iota((slots, tokens), 0) % cap).astype(f32)
    weight_hi = weight.astype(bf16)
    weight_lo = (weight - weight_hi.astype(f32)).astype(bf16)
    share_hi[...] = jnp.where(chosen, nn(owner, weight_hi), 0.0).astype(bf16)
    share_lo[...] = jnp.where(chosen, nn(owner, weight_lo), 0.0).astype(bf16)
    chosen = chosen.astype(f32).astype(bf16)

    loads[1].wait()
    order = (
        iota((positions, positions), 1)
        == (iota((positions, positions), 0) % CHUNKS) * steps
        + iota((positions, positions), 0) // CHUNKS
    ).astype(f32).astype(bf16)
    order_t = (
        iota((positions, positions), 0)
        == (iota((positions, positions), 1) % CHUNKS) * steps
        + iota((positions, positions), 1) // CHUNKS
    ).astype(f32).astype(bf16)
    step = step_in[...]
    groups = step.shape[0]
    high = step.astype(bf16).astype(f32)
    middle = (step - high).astype(bf16).astype(f32)
    low = step - high - middle
    parts = [high, middle, low]
    padded = -(-3 * groups // 16) * 16
    if padded > 3 * groups:
        parts.append(jnp.zeros((padded - 3 * groups, positions), f32))
    split = jnp.concatenate(parts, axis=0).astype(bf16)
    split = nn(split, order_t).astype(bf16)
    for t in range(tiles):
        lanes = slice(t * tile, (t + 1) * tile)
        source = iota((padded, tile), 0)
        pick = jnp.logical_and(
            source % groups == iota((padded, tile), 1) // states + t * (tile // states),
            source < 3 * groups,
        )
        a_re[:, lanes] = tn(split, pick.astype(f32).astype(bf16))

    for copy in stat_copies:
        copy.wait_recv()
    total = mine_stats[...]
    for k in range(1, count_tp):
        total = total + slot_stats[k]
    total = total.T

    loads[11].wait()
    normed = normalize(b_in[...], total[:tokens], gain_b[...], width).astype(bf16)
    outgoing[...] = nn(chosen, normed).astype(bf16)
    arrivals = [None]
    for k in range(1, count_ep):
        here = pl.ds(k * cap, cap)
        arrivals.append(
            send(
                outgoing.at[here], rows_x.at[here, my_cols], aa_s.at[k], aa_r.at[k],
                ep=partner(me, k),
            )
        )
    rows_x[0:cap, my_cols] = outgoing[0:cap, :]

    per_group = count_ep // groups_y
    group_rows = per_group * cap
    y_arrivals, sib_arrivals = {}, []

    def core_cols(offset):
        owner_tp = lax.rem(my_y + count_y - offset, count_y) * CORES + my_core
        return pl.ds(pl.multiple_of(owner_tp * feats, 128), feats)

    def to_sibling(offset, g):
        here = rows_x.at[pl.ds(g * group_rows, group_rows), core_cols(offset)]
        sib_arrivals.append((g, send(here, here, ds_s.at[offset, g], ds_r.at[offset, g], tp=sibling)))

    def forward(g):
        for k in range(max(1, g * per_group), (g + 1) * per_group):
            arrivals[k].wait_recv()
        here = rows_x.at[pl.ds(g * group_rows, group_rows), my_cols]
        for k in range(1, count_y):
            y_arrivals[k, g] = send(
                here, here, dy_s.at[k, g], dy_r.at[k, g],
                tp=lax.rem(my_y + k, count_y) * CORES + my_core,
            )
        to_sibling(0, g)

    def forward_again(g):
        for k in range(1, count_y):
            y_arrivals[k, g].wait_recv()
            to_sibling(k, g)

    forward(0)

    loads[2].wait()
    normed = normalize(a_in[...], total[tokens:], gain_a[...], width).astype(bf16)
    normed = nn(order, normed).astype(bf16)
    loads[3].wait()
    for i in (4, 5, 6, 7):
        loads[i].wait()
    block = min(32, positions)

    def first_half(t):
        lanes = slice(t * tile, (t + 1) * tile)
        table = slice(t * tile_ch, (t + 1) * tile_ch)
        piece = normed[:, table]
        u_re[:, lanes] = nn(piece, spread(in_re[table, :], group_ch, tile, states))
        u_im[:, lanes] = nn(piece, spread(in_im[table, :], group_ch, tile, states))
        p_re, p_im = pole_in[0:1, lanes], pole_in[1:2, lanes]
        d_re, d_im = pole_in[2:3, lanes], pole_in[3:4, lanes]

        def elementwise(i, passed):
            here = pl.ds(pl.multiple_of(i * block, block), block)
            delta = a_re[here, lanes]
            for j in range(block // CHUNKS):
                passed = passed + delta[j * CHUNKS : (j + 1) * CHUNKS]
            magnitude = jnp.exp(p_re * delta)
            sine, cosine = sin_cos(p_im * delta)
            ab_re = magnitude * cosine
            ab_im = magnitude * sine
            numer = ab_re - 1.0
            k_re = numer * d_re + ab_im * d_im
            k_im = ab_im * d_re - numer * d_im
            v_re, v_im = u_re[here, lanes], u_im[here, lanes]
            a_re[here, lanes] = ab_re
            a_im[here, lanes] = ab_im
            u_re[here, lanes] = k_re * v_re - k_im * v_im
            u_im[here, lanes] = k_re * v_im + k_im * v_re
            return passed

        passed = lax.fori_loop(
            0, positions // block, elementwise, jnp.zeros((CHUNKS, tile), f32)
        )
        magnitude = jnp.exp(p_re * passed)
        sine, cosine = sin_cos(p_im * passed)
        sums[0, :, lanes] = magnitude * cosine
        sums[1, :, lanes] = magnitude * sine

    span = min(1024, flat)

    def chunk_sums(base):
        lanes = slice(base, base + span)

        def one(s, carried):
            s_re, s_im = carried
            here = pl.ds(pl.multiple_of(s * CHUNKS, CHUNKS), CHUNKS)
            b_re, b_im = a_re[here, lanes], a_im[here, lanes]
            return (
                b_re * s_re - b_im * s_im + u_re[here, lanes],
                b_re * s_im + b_im * s_re + u_im[here, lanes],
            )

        zero = jnp.zeros((CHUNKS, span), f32)
        sums[2, :, lanes], sums[3, :, lanes] = lax.fori_loop(0, steps, one, (zero, zero), unroll=2)

    work = [functools.partial(first_half, t) for t in range(tiles)]
    work += [functools.partial(chunk_sums, base) for base in range(0, flat, span)]
    early = groups_y // 2
    for n, do in enumerate(work):
        do()
        if n + 1 < early:
            forward(n + 1)
        if 0 <= n - 1 < early:
            forward_again(n - 1)
    done = len(work)
    for g in range(done + 1, early):
        forward(g)
    for g in range(max(0, done - 1), early):
        forward_again(g)

    def chunk(index, c):
        return sums[index, c : c + 1, :]

    c_re, c_im, s_re, s_im = (chunk(index, 0) for index in range(4))
    for c in range(1, CHUNKS):
        b_re, b_im = chunk(0, c), chunk(1, c)
        c_re, c_im = b_re * c_re - b_im * c_im, b_re * c_im + b_im * c_re
        s_re, s_im = (
            b_re * s_re - b_im * s_im + chunk(2, c),
            b_re * s_im + b_im * s_re + chunk(3, c),
        )
    mine_state[0:1, :] = c_re
    mine_state[1:2, :] = c_im
    mine_state[2:3, :] = s_re
    mine_state[3:4, :] = s_im
    state_copies = [
        send(mine_state, slot_state.at[me], hs_s.at[k], hs_r.at[k], ep=partner(me, k))
        for k in range(1, count_ep)
    ]

    expert_half = slots // halves
    columns = min(256, hid)
    out_columns = min(256, feats)
    groups_half = groups_y // halves

    def hidden_units(h, between):
        top = pl.ds(h * expert_half, expert_half)
        for n in range(hid // columns):
            cols = slice(n * columns, (n + 1) * columns)
            gate = nn(rows_x[top, :], w_gate[:, cols])
            up = nn(rows_x[top, :], w_up[:, cols])
            hidden[top, cols] = (gate * jax.nn.sigmoid(gate) * up).astype(bf16)
            between(n)

    sib_copies, y_copies = {}, {}

    def down(h, target_tp, store):
        top = slice(h * expert_half, (h + 1) * expert_half)
        for n in range(feats // out_columns):
            first = pl.multiple_of(target_tp * feats + n * out_columns, 128)
            store(
                top, slice(n * out_columns, (n + 1) * out_columns),
                nn(hidden[top, :], w_down[:, pl.ds(first, out_columns)]),
            )

    def give_back(h):
        top = slice(h * expert_half, (h + 1) * expert_half)
        for offset in list(range(1, count_y)) + [0]:
            yt = lax.rem(my_y + offset, count_y) * CORES

            def to_send(rows, cols, value, offset=offset):
                sib_send[offset, rows, cols] = value.astype(bf16)

            def to_own(rows, cols, value):
                own[rows, cols] = value

            down(h, yt + 1 - my_core, to_send)
            window = pl.ds(h * expert_half, expert_half)
            sib_copies[h, offset] = send(
                sib_send.at[offset, window], sib_recv.at[offset, window],
                rs_s.at[offset, h], rs_r.at[offset, h], tp=sibling,
            )
            down(h, yt + my_core, to_own)
            if offset == 0:
                continue
            sib_copies[h, offset].wait_recv()
            y_send[offset, top, :] = (
                own[top, :] + sib_recv[offset, top, :].astype(f32)
            ).astype(bf16)
            for g in range(h * groups_half, (h + 1) * groups_half):
                window = pl.ds(g * group_rows, group_rows)
                y_copies[offset, g] = send(
                    y_send.at[offset, window], y_recv.at[offset, window],
                    ry_s.at[offset, g], ry_r.at[offset, g], tp=yt + my_core,
                )

    back_copies = {}

    def finish(g):
        window = slice(g * group_rows, (g + 1) * group_rows)
        total = own[window, :] + sib_recv[0, window, :].astype(f32)
        for offset in range(1, count_y):
            y_copies[offset, g].wait_recv()
            total = total + y_recv[offset, window, :].astype(f32)
        total = total.astype(bf16)
        final[window, :] = total
        if g == 0:
            returned[0:cap, :] = total[0:cap]
        for k in range(max(1, g * per_group), (g + 1) * per_group):
            here = pl.ds(k * cap, cap)
            back_copies[k] = send(
                final.at[here], returned.at[here], ra_s.at[k], ra_r.at[k], ep=partner(me, k)
            )

    def rows_ready(low, high):
        for g, copy in list(sib_arrivals):
            if low <= g < high:
                copy.wait_recv()

    loads[14].wait()
    loads[15].wait()
    rows_ready(0, early)

    def forwards(n):
        if early + n < groups_y:
            forward(early + n)

    hidden_units(0, forwards)
    for g in range(early + hid // columns, groups_y):
        forward(g)
    loads[16].wait()
    give_back(0)
    for g in range(early, groups_y):
        forward_again(g)

    for copy in state_copies:
        copy.wait_recv()

    def fold(q, carried):
        h_re, h_im = carried
        b_re, b_im = slot_state[q, 0:1, :], slot_state[q, 1:2, :]
        return (
            b_re * h_re - b_im * h_im + slot_state[q, 2:3, :],
            b_re * h_im + b_im * h_re + slot_state[q, 3:4, :],
        )

    blank = jnp.zeros((1, flat), f32)
    h_re, h_im = lax.fori_loop(0, me, fold, (blank, blank))
    for c in range(CHUNKS):
        enter[0, c : c + 1, :] = h_re
        enter[1, c : c + 1, :] = h_im
        b_re, b_im = chunk(0, c), chunk(1, c)
        h_re, h_im = (
            b_re * h_re - b_im * h_im + chunk(2, c),
            b_re * h_im + b_im * h_re + chunk(3, c),
        )
    for base in range(0, flat, span):
        lanes = slice(base, base + span)

        def advance(s, carried, lanes=lanes):
            s_re, s_im = carried
            found_re, found_im = [], []
            for j in range(2):
                here = pl.ds(pl.multiple_of(s * 2 * CHUNKS + j * CHUNKS, CHUNKS), CHUNKS)
                b_re, b_im = a_re[here, lanes], a_im[here, lanes]
                s_re, s_im = (
                    b_re * s_re - b_im * s_im + u_re[here, lanes],
                    b_re * s_im + b_im * s_re + u_im[here, lanes],
                )
                found_re.append(s_re)
                found_im.append(s_im)
            both = pl.ds(pl.multiple_of(s * 2 * CHUNKS, 2 * CHUNKS), 2 * CHUNKS)
            n_re[both, lanes] = jnp.concatenate(found_re, axis=0).astype(bf16)
            n_im[both, lanes] = jnp.concatenate(found_im, axis=0).astype(bf16)
            return s_re, s_im

        lax.fori_loop(0, steps // 2, advance, (enter[0, :, lanes], enter[1, :, lanes]))
    for t in range(tiles):
        lanes = slice(t * tile, (t + 1) * tile)
        table = slice(t * tile_ch, (t + 1) * tile_ch)
        response = nt(n_re[:, lanes], spread(rd_re[table, :], group_ch, tile, states)) - nt(
            n_im[:, lanes], spread(rd_im[table, :], group_ch, tile, states)
        )
        mixed[:, table] = jax.nn.gelu(response).astype(bf16)
    mixed_cols = pl.ds(pl.multiple_of(tp * channels, 128), channels)
    mixed_all[:, mixed_cols] = nn(order_t, mixed[...]).astype(bf16)

    def mixed_window(offset):
        owner_tp = lax.rem(my_y + count_y - offset, count_y) * CORES + my_core
        return mixed_all.at[:, pl.ds(pl.multiple_of(owner_tp * channels, 128), channels)]

    mixed_y = {}
    for k in range(1, count_y):
        mixed_y[k] = send(
            mixed_window(0), mixed_window(0), my_s.at[k], my_r.at[k],
            tp=lax.rem(my_y + k, count_y) * CORES + my_core,
        )
    mixed_sib = [send(mixed_window(0), mixed_window(0), ms_s.at[0], ms_r.at[0], tp=sibling)]

    if halves > 1:
        rows_ready(early, groups_y)
        hidden_units(1, lambda n: None)
    for k in range(1, count_y):
        mixed_y[k].wait_recv()
        mixed_sib.append(
            send(mixed_window(k), mixed_window(k), ms_s.at[k], ms_r.at[k], tp=sibling)
        )
    if halves > 1:
        sib_copies[0, 0].wait_recv()
        for g in range(groups_half):
            finish(g)
        give_back(1)

    loads[8].wait()
    loads[9].wait()
    for copy in mixed_sib:
        copy.wait_recv()
    out_a_cols = min(256, out_a.shape[1])
    for n in range(out_a.shape[1] // out_a_cols):
        cols = slice(n * out_a_cols, (n + 1) * out_a_cols)
        value = nn(mixed_all[...], w_value[:, cols])
        gate = nn(mixed_all[...], w_gate_out[:, cols])
        out_a[:, cols] = (value * jax.nn.sigmoid(gate)).astype(bf16)

    sib_copies[halves - 1, 0].wait_recv()
    for g in range(groups_half * (halves - 1), groups_y):
        finish(g)
    for k in range(1, count_ep):
        back_copies[k].wait_recv()
    out_b[...] = (tn(share_hi[...], returned[...]) + tn(share_lo[...], returned[...])).astype(bf16)
    for copy in pending:
        copy.wait_send()


def fused(args, state_size, capacity):
    count_ep, count_tp = lax.axis_size("ep"), lax.axis_size("tp")
    count_y = count_tp // CORES
    positions, channels = args[0].shape
    groups = args[1].shape[0]
    tokens, feats = args[10].shape
    flat = args[3].shape[1]
    slots = count_ep * capacity
    hid = args[14].shape[1]
    width = feats * count_tp
    groups_y, halves = min(count_ep, 8), 2
    dma = pltpu.SemaphoreType.DMA
    vmem = pltpu.VMEM
    scratch = [vmem(x.shape, x.dtype) for x in args] + [
        vmem((8, tokens + positions), f32),
        vmem((count_tp, 8, tokens + positions), f32),
        vmem((slots, feats), bf16),
        vmem((slots, width), bf16),
        vmem((slots, tokens), bf16),
        vmem((slots, tokens), bf16),
        vmem((positions, flat), f32),
        vmem((positions, flat), f32),
        vmem((positions, flat), f32),
        vmem((positions, flat), f32),
        vmem((4, CHUNKS, flat), f32),
        vmem((2, CHUNKS, flat), f32),
        vmem((4, flat), f32),
        vmem((count_ep, 4, flat), f32),
        vmem((positions, flat), bf16),
        vmem((positions, flat), bf16),
        vmem((positions, channels), bf16),
        vmem((positions, channels * count_tp), bf16),
        vmem((slots, hid), bf16),
        vmem((slots, feats), f32),
        vmem((count_y, slots, feats), bf16),
        vmem((count_y, slots, feats), bf16),
        vmem((count_y, slots, feats), bf16),
        vmem((count_y, slots, feats), bf16),
        vmem((slots, feats), bf16),
        vmem((slots, feats), bf16),
        dma((len(args),)),
        dma((count_tp,)), dma((count_tp,)),
        dma((count_ep,)), dma((count_ep,)),
        dma((count_y, groups_y)), dma((count_y, groups_y)),
        dma((count_y, groups_y)), dma((count_y, groups_y)),
        dma((count_ep,)), dma((count_ep,)),
        dma((count_y,)), dma((count_y,)),
        dma((count_y,)), dma((count_y,)),
        dma((count_y, halves)), dma((count_y, halves)),
        dma((count_y, groups_y)), dma((count_y, groups_y)),
        dma((count_ep,)), dma((count_ep,)),
    ]
    return pl.pallas_call(
        functools.partial(kernel, (count_ep, count_tp, groups_y, halves, state_size)),
        out_shape=[
            jax.ShapeDtypeStruct((positions, args[8].shape[1]), bf16),
            jax.ShapeDtypeStruct((tokens, feats), bf16),
        ],
        in_specs=[pl.BlockSpec(memory_space=pl.ANY)] * len(args),
        out_specs=[pl.BlockSpec(memory_space=pltpu.VMEM)] * 2,
        scratch_shapes=scratch,
        compiler_params=pltpu.CompilerParams(
            collective_id=0, has_side_effects=True, vmem_limit_bytes=60 * 1024 * 1024
        ),
    )(*args)


def shards(
    mixer_input, mixer_gain, time_step, pole_real, pole_imag, input_real, input_imag,
    read_real, read_imag, out_value, out_gate, expert_input, expert_gain, routes,
    route_weight, expert_gate, expert_up, expert_down,
):
    tokens, top = routes.shape
    capacity = 2 * top * tokens // lax.axis_size("ep")
    flat_real = pole_real.reshape(-1)
    flat_imag = pole_imag.reshape(-1)
    denom = flat_real * flat_real + flat_imag * flat_imag
    pole = jnp.stack([flat_real, flat_imag, flat_real / denom, flat_imag / denom])

    def by_channel(table):
        return jnp.swapaxes(table, 1, 2).reshape(-1, table.shape[1])

    args = (
        mixer_input, time_step.T, mixer_gain[None, :], pole,
        by_channel(input_real), by_channel(input_imag),
        read_real.reshape(-1, read_real.shape[2]), read_imag.reshape(-1, read_imag.shape[2]),
        out_value, out_gate, expert_input, expert_gain[None, :], routes.T, route_weight.T,
        expert_gate[0], expert_up[0], expert_down[0],
    )
    return tuple(fused(args, pole_real.shape[1], capacity))


def solution(mesh):
    return jax.shard_map(
        shards,
        mesh=mesh,
        in_specs=(
            P("ep", "tp"), P("tp"), P("ep", "tp"), P("tp", None), P("tp", None),
            P("tp", None, None), P("tp", None, None), P("tp", None, None), P("tp", None, None),
            P(None, "tp"), P(None, "tp"), P("ep", "tp"), P("tp"), P("ep", None), P("ep", None),
            P("ep", None, "tp"), P("ep", None, "tp"), P("ep", "tp", None),
        ),
        out_specs=(P("ep", "tp"), P("ep", "tp")),
        check_vma=False,
    )
```

time: 140 us -> 65.8 us (0.47)
  waiting for transfers between devices: 46.8 us -> 0 us
  Pallas kernels: 19.7 us -> 59.3 us
  matrix products: 22.8 us -> 0 us
  blocking collectives: 20.5 us -> 0 us
  between operations: 14 us -> 0.64 us
  starting transfers between devices: 5.63 us -> 0 us
  local copies, waits for them, and re-layouts: 8 us -> 4.83 us
    pallas_call x2 -> x1, Pallas kernels: 19.7 us -> 59.3 us  [fused(): pl.pallas_call(functools.partial(kernel, (count_ep, count_tp, groups_y, h...]
    reduce_scatter x1 -> x0, waiting for transfers between devices: 30.6 us -> none  [shards(): lax.psum_scatter(lax.dot_general(down_weight, hidden, (((0,), (1,)), ((),...]
    dot_general x7 -> x0, matrix products: 22.8 us -> none  [the longest x1 10.5 us: shards(): lax.dot_general(down_weight, hidden, (((0,), (1,)), ((), ())), preferred_...]
    all_to_all x1 -> x0, blocking collectives: 20.5 us -> none  [shards(): lax.all_to_all(outgoing, 'ep', split_axis=0, concat_axis=0, tiled=True)]
    all_gather x2 -> x0, waiting for transfers between devices: 15.5 us -> none  [the longest x1 12.6 us: shards(): piece = lax.all_gather(mixed, 'tp', axis=1, tiled=True)]
    all_to_all x1 -> x0, starting transfers between devices: 5.51 us -> none  [shards(): lax.all_to_all(summed, 'ep', split_axis=1, concat_axis=1, tiled=True)]
    unnamed x36 -> x2, local copies, waits for them, and re-layouts: 7.14 us -> 3.24 us
    another operation x2, local copies, waits for them, and re-layouts: 0.16 us -> 1.59 us  [shards(): jnp.stack([flat_real, flat_imag, flat_real / denom, flat_imag / denom])]
  transfers between devices with their start and end apart: 4 -> 0, of which waited for: 3 -> 0; matrix products, arithmetic and copies ran while one was open for 4% -> 0% of each run, Pallas kernels for 10% -> 0%
where the time goes in v1:
time: 65.8 us; the launch traced here: 65.5 us
  Pallas kernels  59.3 us (90%)
  local copies, waits for them, and re-layouts  4.83 us (7%)
    pallas_call x1, Pallas kernels, fused(): pl.pallas_call(functools.partial(kernel, (count_ep, count_tp, groups_y, h...  59.3 us
    unnamed x2, local copies, waits for them, and re-layouts  3.24 us
    another operation x2, local copies, waits for them, and re-layouts, shards(): jnp.stack([flat_real, flat_imag, flat_real / denom, flat_imag / denom])  1.59 us

profile of v1, /device:TPU:0, one launch (start us, length us, event | category | flops | bytes accessed | tf_op | source)
XLA Modules:
  0.0 65.5 jit_solution(11173663869763980345)
XLA Ops:
  0.6 0.8 %stack_reshape.6 = f32[1,1024]{1,0:T(1,128)S(1)} reshape(f32[32,32]{1,0:T(8,128)} %param.21) | data formatting | bytes 8192 | tf_op jit(solution)/shard_map/stack;reshape | solution.py:641
  1.4 0.8 %stack_reshape.7 = f32[1,1024]{1,0:T(1,128)S(1)} reshape(f32[32,32]{1,0:T(8,128)} %param.22) | data formatting | bytes 8192 | tf_op jit(solution)/shard_map/stack;reshape | solution.py:641
  2.2 0.6 pad_maximum_fusion.refs_3_
  2.9 59.3 %shard_map.185 = (bf16[256,512]{1,0:T(8,128)(2,1)}, bf16[128,512]{1,0:T(8,128)(2,1)}) custom-call(bf16[256,512]{1,0:T(8,128)(2,1)} %refs_0_.1, f32[32,256]{1,0:T(8,128)} %bitcast.23, f32[1,512]{1,0:T(1,128)} %bitcast.24, f32[4,1024]{1,0:T(4,128)} %pad_maximum_fusion.refs_3_, f32[512,32]{1,0:T(8,128)} %bitcast.19, f32[512,32]{1,0:T(8,128)} %bitcast.20, ...), custom_call_target="tpu_custom_call" | custom-call | tf_op jit(solution)/shard_map/pallas_call | solution.py:616
  62.2 1.7 %copy.22 = bf16[256,512]{1,0:T(8,128)(2,1)} copy(bf16[256,512]{1,0:T(8,128)(2,1)} %get-tuple-element.6) | data formatting | bytes 524288
  63.9 1.6 %copy.23 = bf16[128,512]{1,0:T(8,128)(2,1)} copy(bf16[128,512]{1,0:T(8,128)(2,1)} %get-tuple-element.7) | data formatting | bytes 262144
  (1 shorter events, 0.0 us)

commit v2 on v1

--- a/solution.py
+++ b/solution.py
@@ -86,19 +86,19 @@
 
 def kernel(dims, *refs):
     count_ep, count_tp, groups_y, halves, state_size = dims
-    hbm, refs = refs[:17], refs[17:]
+    hbm, refs = refs[:18], refs[18:]
     (out_a, out_b), refs = refs[:2], refs[2:]
-    vm, refs = refs[:17], refs[17:]
+    vm, refs = refs[:18], refs[18:]
     (
-        mine_stats, slot_stats, outgoing, rows_x, share_hi, share_lo, a_re, a_im, u_re, u_im,
+        mine_stats, slot_stats, pole, tokens_far, routes_far, gain_all, rows_n, outgoing, rows_x, share_hi, share_lo, a_re, a_im, u_re, u_im,
         sums, enter, mine_state, slot_state, n_re, n_im, mixed, mixed_all, hidden, own,
         sib_send, sib_recv, y_send, y_recv, final, returned,
-        sem_in, st_s, st_r, aa_s, aa_r, dy_s, dy_r, ds_s, ds_r, hs_s, hs_r,
+        sem_in, far_s, far_r, gn_s, gn_r, st_s, st_r, aa_s, aa_r, dy_s, dy_r, ds_s, ds_r, hs_s, hs_r,
         my_s, my_r, ms_s, ms_r, rs_s, rs_r, ry_s, ry_r, ra_s, ra_r,
     ) = refs
     (
-        a_in, step_in, gain_a, pole_in, in_re, in_im, rd_re, rd_im, w_value, w_gate_out,
-        b_in, gain_b, routes_in, weight_in, w_gate, w_up, w_down,
+        a_in, step_in, gain_a, real_in, in_re, in_im, rd_re, rd_im, w_value, w_gate_out,
+        b_in, gain_b, routes_in, weight_in, w_gate, w_up, w_down, imag_in,
     ) = vm
 
     me = lax.axis_index("ep")
@@ -123,7 +123,7 @@
         pltpu.make_async_copy(source, target, sem_in.at[i])
         for i, (source, target) in enumerate(zip(hbm, vm))
     ]
-    for i in (10, 0, 12, 13, 11, 1, 3, 2, 4, 5, 6, 7, 14, 15, 16, 8, 9):
+    for i in (10, 12, 11, 0, 1, 3, 17, 2, 13, 4, 5, 6, 7, 14, 15, 16, 8, 9):
         loads[i].start()
 
     pending = []
@@ -153,41 +153,96 @@
     expert_rows = max(16, count_ep)
     my_cols = pl.ds(pl.multiple_of(tp * feats, 128), feats)
 
-    loads[10].wait()
+    portal = partner(me, count_ep // 2)
+    for i in (12, 11, 10):
+        loads[i].wait()
+    pl.semaphore_wait(barrier, count_ep + count_tp - 2)
+    far_routes = send(routes_in, routes_far, far_s.at[0], far_r.at[0], ep=portal)
+    far_tokens = send(b_in, tokens_far, far_s.at[1], far_r.at[1], ep=portal)
+    gain_copies = [
+        send(
+            gain_b, gain_all.at[:, my_cols], gn_s.at[k], gn_r.at[k], tp=lax.rem(tp + k, count_tp)
+        )
+        for k in range(1, count_tp)
+    ]
+    gain_all[:, my_cols] = gain_b[...]
+    near = count_ep // 2
+    expert_of = iota((expert_rows, tokens), 0)
+    before = (iota((tokens, tokens), 0) < iota((tokens, tokens), 1)).astype(bf16)
+
+    def places(routes):
+        hit = jnp.zeros((expert_rows, tokens), jnp.bool_)
+        for k in range(routes.shape[0]):
+            hit = jnp.logical_or(hit, routes[k : k + 1, :] == expert_of)
+        place = nn(hit.astype(f32).astype(bf16), before)
+        return jnp.where(hit, place, -1.0).astype(bf16)
+
+    def owners(low, high):
+        return jnp.concatenate(
+            [
+                (iota((cap, expert_rows), 1) == partner(me, k)).astype(f32)
+                for k in range(low, high)
+            ],
+            axis=0,
+        ).astype(bf16)
+
+    def select(owner, place):
+        return nn(owner, place) == (iota((owner.shape[0], tokens), 0) % cap).astype(f32)
+
+    place_own = places(routes_in[...])
+    owner_near = owners(0, near)
+    chosen_near = select(owner_near, place_own)
+    chosen = chosen_near.astype(f32).astype(bf16)
+
+    arrivals = {}
+
+    def hand_out(base, values):
+        outgoing[base * cap : (base + near) * cap, :] = values
+        for k in range(1, near):
+            here = pl.ds((base + k) * cap, cap)
+            arrivals[base + k] = send(
+                outgoing.at[here], rows_x.at[here, my_cols], aa_s.at[base + k],
+                aa_r.at[base + k], ep=partner(me, k),
+            )
+        rows_x[base * cap : (base + 1) * cap, my_cols] = values[0:cap]
+
+    per_group = count_ep // groups_y
+    group_rows = per_group * cap
+    y_arrivals, sib_arrivals = {}, []
+
+    def core_cols(offset):
+        owner_tp = lax.rem(my_y + count_y - offset, count_y) * CORES + my_core
+        return pl.ds(pl.multiple_of(owner_tp * feats, 128), feats)
+
+    def to_sibling(offset, g):
+        here = rows_x.at[pl.ds(g * group_rows, group_rows), core_cols(offset)]
+        sib_arrivals.append((g, send(here, here, ds_s.at[offset, g], ds_r.at[offset, g], tp=sibling)))
+
+    def forward(g):
+        for k in range(g * per_group, (g + 1) * per_group):
+            if k in arrivals:
+                arrivals[k].wait_recv()
+        here = rows_x.at[pl.ds(g * group_rows, group_rows), my_cols]
+        for k in range(1, count_y):
+            y_arrivals[k, g] = send(
+                here, here, dy_s.at[k, g], dy_r.at[k, g],
+                tp=lax.rem(my_y + k, count_y) * CORES + my_core,
+            )
+        to_sibling(0, g)
+
+    def forward_again(g):
+        for k in range(1, count_y):
+            y_arrivals[k, g].wait_recv()
+            to_sibling(k, g)
+
+    hand_out(0, nn(chosen, b_in[...]).astype(bf16))
+    forward(0)
     loads[0].wait()
-    mine_stats[:, :tokens] = row_sums(b_in[...])
-    mine_stats[:, tokens:] = row_sums(a_in[...])
-    pl.semaphore_wait(barrier, count_ep + count_tp - 2)
+    mine_stats[...] = row_sums(a_in[...])
     stat_copies = [
         send(mine_stats, slot_stats.at[k], st_s.at[k], st_r.at[k], tp=lax.rem(tp + k, count_tp))
         for k in range(1, count_tp)
     ]
-
-    loads[12].wait()
-    loads[13].wait()
-    expert_of = iota((expert_rows, tokens), 0)
-    hit = jnp.zeros((expert_rows, tokens), jnp.bool_)
-    weight = jnp.zeros((expert_rows, tokens), f32)
-    for k in range(routes_in.shape[0]):
-        this = routes_in[k : k + 1, :] == expert_of
-        hit = jnp.logical_or(hit, this)
-        weight = jnp.where(this, weight_in[k : k + 1, :], weight)
-    before = (iota((tokens, tokens), 0) < iota((tokens, tokens), 1)).astype(bf16)
-    place = nn(hit.astype(f32).astype(bf16), before)
-    place = jnp.where(hit, place, -1.0).astype(bf16)
-    owner = jnp.concatenate(
-        [
-            (iota((cap, expert_rows), 1) == partner(me, k)).astype(f32)
-            for k in range(count_ep)
-        ],
-        axis=0,
-    ).astype(bf16)
-    chosen = nn(owner, place) == (iota((slots, tokens), 0) % cap).astype(f32)
-    weight_hi = weight.astype(bf16)
-    weight_lo = (weight - weight_hi.astype(f32)).astype(bf16)
-    share_hi[...] = jnp.where(chosen, nn(owner, weight_hi), 0.0).astype(bf16)
-    share_lo[...] = jnp.where(chosen, nn(owner, weight_lo), 0.0).astype(bf16)
-    chosen = chosen.astype(f32).astype(bf16)
 
     loads[1].wait()
     order = (
@@ -220,73 +275,31 @@
         )
         a_re[:, lanes] = tn(split, pick.astype(f32).astype(bf16))
 
-    for copy in stat_copies:
-        copy.wait_recv()
-    total = mine_stats[...]
-    for k in range(1, count_tp):
-        total = total + slot_stats[k]
-    total = total.T
-
-    loads[11].wait()
-    normed = normalize(b_in[...], total[:tokens], gain_b[...], width).astype(bf16)
-    outgoing[...] = nn(chosen, normed).astype(bf16)
-    arrivals = [None]
-    for k in range(1, count_ep):
-        here = pl.ds(k * cap, cap)
-        arrivals.append(
-            send(
-                outgoing.at[here], rows_x.at[here, my_cols], aa_s.at[k], aa_r.at[k],
-                ep=partner(me, k),
-            )
-        )
-    rows_x[0:cap, my_cols] = outgoing[0:cap, :]
-
-    per_group = count_ep // groups_y
-    group_rows = per_group * cap
-    y_arrivals, sib_arrivals = {}, []
-
-    def core_cols(offset):
-        owner_tp = lax.rem(my_y + count_y - offset, count_y) * CORES + my_core
-        return pl.ds(pl.multiple_of(owner_tp * feats, 128), feats)
-
-    def to_sibling(offset, g):
-        here = rows_x.at[pl.ds(g * group_rows, group_rows), core_cols(offset)]
-        sib_arrivals.append((g, send(here, here, ds_s.at[offset, g], ds_r.at[offset, g], tp=sibling)))
-
-    def forward(g):
-        for k in range(max(1, g * per_group), (g + 1) * per_group):
-            arrivals[k].wait_recv()
-        here = rows_x.at[pl.ds(g * group_rows, group_rows), my_cols]
-        for k in range(1, count_y):
-            y_arrivals[k, g] = send(
-                here, here, dy_s.at[k, g], dy_r.at[k, g],
-                tp=lax.rem(my_y + k, count_y) * CORES + my_core,
-            )
-        to_sibling(0, g)
-
-    def forward_again(g):
-        for k in range(1, count_y):
-            y_arrivals[k, g].wait_recv()
-            to_sibling(k, g)
-
-    forward(0)
-
-    loads[2].wait()
-    normed = normalize(a_in[...], total[tokens:], gain_a[...], width).astype(bf16)
-    normed = nn(order, normed).astype(bf16)
     loads[3].wait()
-    for i in (4, 5, 6, 7):
-        loads[i].wait()
+    loads[17].wait()
+    pick = (iota((states, flat), 0) == iota((states, flat), 1) % states).astype(f32).astype(bf16)
+    own_lane = iota((groups, flat), 0) == iota((groups, flat), 1) // states
+
+    def to_lanes(table):
+        high = table.astype(bf16)
+        rest = table - high.astype(f32)
+        middle = rest.astype(bf16)
+        low = (rest - middle.astype(f32)).astype(bf16)
+        wide = nn(high, pick) + (nn(middle, pick) + nn(low, pick))
+        return jnp.sum(jnp.where(own_lane, wide, 0.0), axis=0, keepdims=True)
+
+    real, imag = to_lanes(real_in[...]), to_lanes(imag_in[...])
+    denom = real * real + imag * imag
+    pole[0:1, :] = real
+    pole[1:2, :] = imag
+    pole[2:3, :] = real / denom
+    pole[3:4, :] = imag / denom
     block = min(32, positions)
 
-    def first_half(t):
+    def steps_of(t):
         lanes = slice(t * tile, (t + 1) * tile)
-        table = slice(t * tile_ch, (t + 1) * tile_ch)
-        piece = normed[:, table]
-        u_re[:, lanes] = nn(piece, spread(in_re[table, :], group_ch, tile, states))
-        u_im[:, lanes] = nn(piece, spread(in_im[table, :], group_ch, tile, states))
-        p_re, p_im = pole_in[0:1, lanes], pole_in[1:2, lanes]
-        d_re, d_im = pole_in[2:3, lanes], pole_in[3:4, lanes]
+        p_re, p_im = pole[0:1, lanes], pole[1:2, lanes]
+        d_re, d_im = pole[2:3, lanes], pole[3:4, lanes]
 
         def elementwise(i, passed):
             here = pl.ds(pl.multiple_of(i * block, block), block)
@@ -298,13 +311,10 @@
             ab_re = magnitude * cosine
             ab_im = magnitude * sine
             numer = ab_re - 1.0
-            k_re = numer * d_re + ab_im * d_im
-            k_im = ab_im * d_re - numer * d_im
-            v_re, v_im = u_re[here, lanes], u_im[here, lanes]
             a_re[here, lanes] = ab_re
             a_im[here, lanes] = ab_im
-            u_re[here, lanes] = k_re * v_re - k_im * v_im
-            u_im[here, lanes] = k_re * v_im + k_im * v_re
+            u_re[here, lanes] = numer * d_re + ab_im * d_im
+            u_im[here, lanes] = ab_im * d_re - numer * d_im
             return passed
 
         passed = lax.fori_loop(
@@ -314,6 +324,35 @@
         sine, cosine = sin_cos(p_im * passed)
         sums[0, :, lanes] = magnitude * cosine
         sums[1, :, lanes] = magnitude * sine
+
+    forward(1)
+    for t in range(tiles):
+        steps_of(t)
+    forward_again(0)
+    far_routes.wait_recv()
+    chosen_far = select(owner_near, places(routes_far[...])).astype(f32).astype(bf16)
+    for copy in stat_copies:
+        copy.wait_recv()
+    total = mine_stats[...]
+    for k in range(1, count_tp):
+        total = total + slot_stats[k]
+    total = total.T
+
+    loads[2].wait()
+    normed = normalize(a_in[...], total, gain_a[...], width).astype(bf16)
+    normed = nn(order, normed).astype(bf16)
+    for i in (4, 5, 6, 7):
+        loads[i].wait()
+
+    def first_half(t):
+        lanes = slice(t * tile, (t + 1) * tile)
+        table = slice(t * tile_ch, (t + 1) * tile_ch)
+        piece = normed[:, table]
+        v_re = nn(piece, spread(in_re[table, :], group_ch, tile, states))
+        v_im = nn(piece, spread(in_im[table, :], group_ch, tile, states))
+        k_re, k_im = u_re[:, lanes], u_im[:, lanes]
+        u_re[:, lanes] = k_re * v_re - k_im * v_im
+        u_im[:, lanes] = k_re * v_im + k_im * v_re
 
     span = min(1024, flat)
 
@@ -332,21 +371,15 @@
         zero = jnp.zeros((CHUNKS, span), f32)
         sums[2, :, lanes], sums[3, :, lanes] = lax.fori_loop(0, steps, one, (zero, zero), unroll=2)
 
-    work = [functools.partial(first_half, t) for t in range(tiles)]
-    work += [functools.partial(chunk_sums, base) for base in range(0, flat, span)]
     early = groups_y // 2
-    for n, do in enumerate(work):
-        do()
-        if n + 1 < early:
-            forward(n + 1)
-        if 0 <= n - 1 < early:
-            forward_again(n - 1)
-    done = len(work)
-    for g in range(done + 1, early):
+    for t in range(tiles // 2):
+        first_half(t)
+    for g in range(2, early):
         forward(g)
-    for g in range(max(0, done - 1), early):
-        forward_again(g)
-
+    for t in range(tiles // 2, tiles):
+        first_half(t)
+    for base in range(0, flat, span):
+        chunk_sums(base)
     def chunk(index, c):
         return sums[index, c : c + 1, :]
 
@@ -367,17 +400,48 @@
         for k in range(1, count_ep)
     ]
 
+    far_tokens.wait_recv()
+    hand_out(near, nn(chosen_far, tokens_far[...]).astype(bf16))
+    forward(early)
+    for g in range(1, early):
+        forward_again(g)
+    loads[13].wait()
+    weight = jnp.zeros((expert_rows, tokens), f32)
+    for k in range(routes_in.shape[0]):
+        this = routes_in[k : k + 1, :] == expert_of
+        weight = jnp.where(this, weight_in[k : k + 1, :], weight)
+    weight_hi = weight.astype(bf16)
+    weight_lo = (weight - weight_hi.astype(f32)).astype(bf16)
+    owner_far = owners(near, count_ep)
+    for rows, owner, here in (
+        (slice(0, near * cap), owner_near, chosen_near),
+        (slice(near * cap, slots), owner_far, select(owner_far, place_own)),
+    ):
+        share_hi[rows, :] = jnp.where(here, nn(owner, weight_hi), 0.0).astype(bf16)
+        share_lo[rows, :] = jnp.where(here, nn(owner, weight_lo), 0.0).astype(bf16)
+
     expert_half = slots // halves
     columns = min(256, hid)
     out_columns = min(256, feats)
     groups_half = groups_y // halves
 
+    def normalize_rows(h):
+        step_rows = min(64, expert_half)
+        for r in range(h * expert_half, (h + 1) * expert_half, step_rows):
+            rows = slice(r, r + step_rows)
+            wide = rows_x[rows, :].astype(f32)
+            average = jnp.sum(wide, axis=1, keepdims=True) / width
+            square = jnp.sum(wide * wide, axis=1, keepdims=True) / width
+            variance = square - average * average
+            wide = (wide - average) * lax.rsqrt(variance + norm_eps) * gain_all[...]
+            rows_n[rows, :] = wide.astype(bf16)
+
     def hidden_units(h, between):
         top = pl.ds(h * expert_half, expert_half)
         for n in range(hid // columns):
             cols = slice(n * columns, (n + 1) * columns)
-            gate = nn(rows_x[top, :], w_gate[:, cols])
-            up = nn(rows_x[top, :], w_up[:, cols])
+            gate = nn(rows_n[top, :], w_gate[:, cols])
+            up = nn(rows_n[top, :], w_up[:, cols])
             hidden[top, cols] = (gate * jax.nn.sigmoid(gate) * up).astype(bf16)
             between(n)
 
@@ -392,9 +456,9 @@
                 nn(hidden[top, :], w_down[:, pl.ds(first, out_columns)]),
             )
 
-    def give_back(h):
+    def give_back(h, offsets):
         top = slice(h * expert_half, (h + 1) * expert_half)
-        for offset in list(range(1, count_y)) + [0]:
+        for offset in offsets:
             yt = lax.rem(my_y + offset, count_y) * CORES
 
             def to_send(rows, cols, value, offset=offset):
@@ -446,22 +510,23 @@
             if low <= g < high:
                 copy.wait_recv()
 
+    rows_ready(0, early)
+    for copy in gain_copies:
+        copy.wait_recv()
+    normalize_rows(0)
+    forward(early + 1)
     loads[14].wait()
     loads[15].wait()
-    rows_ready(0, early)
 
     def forwards(n):
-        if early + n < groups_y:
-            forward(early + n)
+        if early + 2 + n < groups_y:
+            forward(early + 2 + n)
 
     hidden_units(0, forwards)
-    for g in range(early + hid // columns, groups_y):
+    for g in range(early + 2 + hid // columns, groups_y):
         forward(g)
-    loads[16].wait()
-    give_back(0)
-    for g in range(early, groups_y):
-        forward_again(g)
-
+    forward_again(early)
+    forward_again(early + 1)
     for copy in state_copies:
         copy.wait_recv()
 
@@ -526,20 +591,28 @@
         )
     mixed_sib = [send(mixed_window(0), mixed_window(0), ms_s.at[0], ms_r.at[0], tp=sibling)]
 
-    if halves > 1:
-        rows_ready(early, groups_y)
-        hidden_units(1, lambda n: None)
+    for g in range(early + 2, groups_y):
+        forward_again(g)
+    rows_ready(early, groups_y)
+    normalize_rows(1)
+    hidden_units(1, lambda n: None)
+    others = list(range(1, count_y))
+    loads[16].wait()
+    give_back(1, others)
+    give_back(0, others)
+    give_back(1, [0])
+    sib_copies[1, 0].wait_recv()
+    finish(groups_half)
+    give_back(0, [0])
+    for g in range(groups_half + 1, groups_half + 2):
+        finish(g)
     for k in range(1, count_y):
         mixed_y[k].wait_recv()
         mixed_sib.append(
             send(mixed_window(k), mixed_window(k), ms_s.at[k], ms_r.at[k], tp=sibling)
         )
-    if halves > 1:
-        sib_copies[0, 0].wait_recv()
-        for g in range(groups_half):
-            finish(g)
-        give_back(1)
-
+    for g in range(groups_half + 2, groups_y):
+        finish(g)
     loads[8].wait()
     loads[9].wait()
     for copy in mixed_sib:
@@ -550,9 +623,8 @@
         value = nn(mixed_all[...], w_value[:, cols])
         gate = nn(mixed_all[...], w_gate_out[:, cols])
         out_a[:, cols] = (value * jax.nn.sigmoid(gate)).astype(bf16)
-
-    sib_copies[halves - 1, 0].wait_recv()
-    for g in range(groups_half * (halves - 1), groups_y):
+    sib_copies[0, 0].wait_recv()
+    for g in range(groups_half):
         finish(g)
     for k in range(1, count_ep):
         back_copies[k].wait_recv()
@@ -567,7 +639,7 @@
     positions, channels = args[0].shape
     groups = args[1].shape[0]
     tokens, feats = args[10].shape
-    flat = args[3].shape[1]
+    flat = args[3].shape[0] * args[3].shape[1]
     slots = count_ep * capacity
     hid = args[14].shape[1]
     width = feats * count_tp
@@ -575,8 +647,13 @@
     dma = pltpu.SemaphoreType.DMA
     vmem = pltpu.VMEM
     scratch = [vmem(x.shape, x.dtype) for x in args] + [
-        vmem((8, tokens + positions), f32),
-        vmem((count_tp, 8, tokens + positions), f32),
+        vmem((8, positions), f32),
+        vmem((count_tp, 8, positions), f32),
+        vmem((4, flat), f32),
+        vmem((tokens, feats), bf16),
+        vmem(args[12].shape, args[12].dtype),
+        vmem((1, width), f32),
+        vmem((slots, width), bf16),
         vmem((slots, feats), bf16),
         vmem((slots, width), bf16),
         vmem((slots, tokens), bf16),
@@ -602,6 +679,8 @@
         vmem((slots, feats), bf16),
         vmem((slots, feats), bf16),
         dma((len(args),)),
+        dma((2,)), dma((2,)),
+        dma((count_tp,)), dma((count_tp,)),
         dma((count_tp,)), dma((count_tp,)),
         dma((count_ep,)), dma((count_ep,)),
         dma((count_y, groups_y)), dma((count_y, groups_y)),
@@ -616,10 +695,10 @@
     return pl.pallas_call(
         functools.partial(kernel, (count_ep, count_tp, groups_y, halves, state_size)),
         out_shape=[
-            jax.ShapeDtypeStruct((positions, args[8].shape[1]), bf16),
-            jax.ShapeDtypeStruct((tokens, feats), bf16),
+            vmem((positions, args[8].shape[1]), bf16),
+            vmem((tokens, feats), bf16),
         ],
-        in_specs=[pl.BlockSpec(memory_space=pl.ANY)] * len(args),
+        in_specs=[pl.BlockSpec(memory_space=pltpu.HBM)] * len(args),
         out_specs=[pl.BlockSpec(memory_space=pltpu.VMEM)] * 2,
         scratch_shapes=scratch,
         compiler_params=pltpu.CompilerParams(
@@ -635,20 +714,15 @@
 ):
     tokens, top = routes.shape
     capacity = 2 * top * tokens // lax.axis_size("ep")
-    flat_real = pole_real.reshape(-1)
-    flat_imag = pole_imag.reshape(-1)
-    denom = flat_real * flat_real + flat_imag * flat_imag
-    pole = jnp.stack([flat_real, flat_imag, flat_real / denom, flat_imag / denom])
-
     def by_channel(table):
         return jnp.swapaxes(table, 1, 2).reshape(-1, table.shape[1])
 
     args = (
-        mixer_input, time_step.T, mixer_gain[None, :], pole,
+        mixer_input, time_step.T, mixer_gain[None, :], pole_real,
         by_channel(input_real), by_channel(input_imag),
         read_real.reshape(-1, read_real.shape[2]), read_imag.reshape(-1, read_imag.shape[2]),
         out_value, out_gate, expert_input, expert_gain[None, :], routes.T, route_weight.T,
-        expert_gate[0], expert_up[0], expert_down[0],
+        expert_gate[0], expert_up[0], expert_down[0], pole_imag,
     )
     return tuple(fused(args, pole_real.shape[1], capacity))
 

time: 65.8 us -> 53 us (0.81)
  Pallas kernels: 59.3 us -> 50.8 us
  local copies, waits for them, and re-layouts: 4.83 us -> 1.36 us
    pallas_call x1, Pallas kernels: 59.3 us -> 50.8 us  [fused(): pl.pallas_call(functools.partial(kernel, (count_ep, count_tp, groups_y, h...]
    unnamed x2, local copies, waits for them, and re-layouts: 3.24 us -> 1.36 us
    another operation x2 -> x0, local copies, waits for them, and re-layouts: 1.59 us -> none  [shards(): jnp.stack([flat_real, flat_imag, flat_real / denom, flat_imag / denom])]
where the time goes in v2:
time: 53 us; the launch traced here: 52.8 us
  Pallas kernels  50.8 us (96%)
  local copies, waits for them, and re-layouts  1.36 us (3%)
  between operations  0.65 us (1%)
    pallas_call x1, Pallas kernels, fused(): pl.pallas_call(functools.partial(kernel, (count_ep, count_tp, groups_y, h...  50.8 us
    unnamed x2, local copies, waits for them, and re-layouts  1.36 us

profile of v2, /device:TPU:0, one launch (start us, length us, event | category | flops | bytes accessed | tf_op | source)
XLA Modules:
  0.0 52.8 jit_solution(6314038175958086574)
XLA Ops:
  0.6 50.8 %shard_map.185 = (bf16[256,512]{1,0:T(8,128)(2,1)S(1)}, bf16[128,512]{1,0:T(8,128)(2,1)S(1)}) custom-call(bf16[256,512]{1,0:T(8,128)(2,1)} %refs_0_.1, f32[32,256]{1,0:T(8,128)} %bitcast.23, f32[1,512]{1,0:T(1,128)} %bitcast.24, f32[32,32]{1,0:T(8,128)} %refs_3_.1, f32[512,32]{1,0:T(8,128)} %bitcast.19, f32[512,32]{1,0:T(8,128)} %bitcast.20, ...), custom_call_target="tpu_custom_call" | custom-call | tf_op jit(solution)/shard_map/pallas_call | solution.py:695
  51.5 0.7 %copy.22 = bf16[256,512]{1,0:T(8,128)(2,1)} copy(bf16[256,512]{1,0:T(8,128)(2,1)S(1)} %get-tuple-element.2) | data formatting | bytes 524288
  52.2 0.7 %copy.23 = bf16[128,512]{1,0:T(8,128)(2,1)} copy(bf16[128,512]{1,0:T(8,128)(2,1)S(1)} %get-tuple-element.3) | data formatting | bytes 262144

commit v3 on v2

--- a/solution.py
+++ b/solution.py
@@ -85,7 +85,7 @@
 
 
 def kernel(dims, *refs):
-    count_ep, count_tp, groups_y, halves, state_size = dims
+    count_ep, count_tp, groups_y, pieces, state_size = dims
     hbm, refs = refs[:18], refs[18:]
     (out_a, out_b), refs = refs[:2], refs[2:]
     vm, refs = refs[:18], refs[18:]
@@ -158,7 +158,15 @@
         loads[i].wait()
     pl.semaphore_wait(barrier, count_ep + count_tp - 2)
     far_routes = send(routes_in, routes_far, far_s.at[0], far_r.at[0], ep=portal)
-    far_tokens = send(b_in, tokens_far, far_s.at[1], far_r.at[1], ep=portal)
+    cuts = 2 if feats % 256 == 0 else 1
+    cut = [slice(c * feats // cuts, (c + 1) * feats // cuts) for c in range(cuts)]
+    far_tokens = [
+        send(
+            b_in.at[:, cut[c]], tokens_far.at[:, cut[c]], far_s.at[1 + c], far_r.at[1 + c],
+            ep=portal,
+        )
+        for c in range(cuts)
+    ]
     gain_copies = [
         send(
             gain_b, gain_all.at[:, my_cols], gn_s.at[k], gn_r.at[k], tp=lax.rem(tp + k, count_tp)
@@ -196,15 +204,19 @@
 
     arrivals = {}
 
-    def hand_out(base, values):
-        outgoing[base * cap : (base + near) * cap, :] = values
+    def hand_out(base, columns, values, c):
+        outgoing[base * cap : (base + near) * cap, columns] = values
+        size = columns.stop - columns.start
+        there = pl.ds(pl.multiple_of(tp * feats + columns.start, 128), size)
         for k in range(1, near):
             here = pl.ds((base + k) * cap, cap)
-            arrivals[base + k] = send(
-                outgoing.at[here], rows_x.at[here, my_cols], aa_s.at[base + k],
-                aa_r.at[base + k], ep=partner(me, k),
+            arrivals.setdefault(base + k, []).append(
+                send(
+                    outgoing.at[here, columns], rows_x.at[here, there], aa_s.at[c, base + k],
+                    aa_r.at[c, base + k], ep=partner(me, k),
+                )
             )
-        rows_x[base * cap : (base + 1) * cap, my_cols] = values[0:cap]
+        rows_x[base * cap : (base + 1) * cap, there] = values[0:cap]
 
     per_group = count_ep // groups_y
     group_rows = per_group * cap
@@ -220,8 +232,8 @@
 
     def forward(g):
         for k in range(g * per_group, (g + 1) * per_group):
-            if k in arrivals:
-                arrivals[k].wait_recv()
+            for copy in arrivals.get(k, []):
+                copy.wait_recv()
         here = rows_x.at[pl.ds(g * group_rows, group_rows), my_cols]
         for k in range(1, count_y):
             y_arrivals[k, g] = send(
@@ -235,7 +247,7 @@
             y_arrivals[k, g].wait_recv()
             to_sibling(k, g)
 
-    hand_out(0, nn(chosen, b_in[...]).astype(bf16))
+    hand_out(0, slice(0, feats), nn(chosen, b_in[...]).astype(bf16), 0)
     forward(0)
     loads[0].wait()
     mine_stats[...] = row_sums(a_in[...])
@@ -325,12 +337,19 @@
         sums[0, :, lanes] = magnitude * cosine
         sums[1, :, lanes] = magnitude * sine
 
-    forward(1)
     for t in range(tiles):
         steps_of(t)
+    forward(1)
     forward_again(0)
     far_routes.wait_recv()
     chosen_far = select(owner_near, places(routes_far[...])).astype(f32).astype(bf16)
+
+    def hand_out_far(c):
+        far_tokens[c].wait_recv()
+        hand_out(near, cut[c], nn(chosen_far, tokens_far[:, cut[c]]).astype(bf16), c)
+
+    for c in range(cuts - 1):
+        hand_out_far(c)
     for copy in stat_copies:
         copy.wait_recv()
     total = mine_stats[...]
@@ -372,11 +391,7 @@
         sums[2, :, lanes], sums[3, :, lanes] = lax.fori_loop(0, steps, one, (zero, zero), unroll=2)
 
     early = groups_y // 2
-    for t in range(tiles // 2):
-        first_half(t)
-    for g in range(2, early):
-        forward(g)
-    for t in range(tiles // 2, tiles):
+    for t in range(tiles):
         first_half(t)
     for base in range(0, flat, span):
         chunk_sums(base)
@@ -395,16 +410,24 @@
     mine_state[1:2, :] = c_im
     mine_state[2:3, :] = s_re
     mine_state[3:4, :] = s_im
-    state_copies = [
-        send(mine_state, slot_state.at[me], hs_s.at[k], hs_r.at[k], ep=partner(me, k))
-        for k in range(1, count_ep)
-    ]
-
-    far_tokens.wait_recv()
-    hand_out(near, nn(chosen_far, tokens_far[...]).astype(bf16))
+    state_copies = []
+    for k in range(1, count_ep):
+        other = partner(me, k)
+        copy = pltpu.make_async_remote_copy(
+            src_ref=mine_state, dst_ref=slot_state.at[me], send_sem=hs_s.at[k], recv_sem=hs_r.at[k],
+            device_id={"ep": other}, device_id_type=pl.DeviceIdType.MESH,
+        )
+        state_copies.append((other, copy))
+
+        @pl.when(other > me)
+        def _(copy=copy):
+            copy.start()
+
+    hand_out_far(cuts - 1)
     forward(early)
-    for g in range(1, early):
-        forward_again(g)
+    for g in range(2, early - 1):
+        forward(g)
+    forward_again(1)
     loads[13].wait()
     weight = jnp.zeros((expert_rows, tokens), f32)
     for k in range(routes_in.shape[0]):
@@ -420,14 +443,19 @@
         share_hi[rows, :] = jnp.where(here, nn(owner, weight_hi), 0.0).astype(bf16)
         share_lo[rows, :] = jnp.where(here, nn(owner, weight_lo), 0.0).astype(bf16)
 
-    expert_half = slots // halves
     columns = min(256, hid)
     out_columns = min(256, feats)
-    groups_half = groups_y // halves
-
-    def normalize_rows(h):
-        step_rows = min(64, expert_half)
-        for r in range(h * expert_half, (h + 1) * expert_half, step_rows):
+    middle = early + (groups_y - early) // 2
+    split = early // 2
+    blocks = ((0, split), (early, middle), (middle, groups_y), (split, early))
+
+    def rows_of(b):
+        return slice(blocks[b][0] * group_rows, blocks[b][1] * group_rows)
+
+
+    def normalize_rows(b):
+        step_rows = min(64, group_rows)
+        for r in range(rows_of(b).start, rows_of(b).stop, step_rows):
             rows = slice(r, r + step_rows)
             wide = rows_x[rows, :].astype(f32)
             average = jnp.sum(wide, axis=1, keepdims=True) / width
@@ -436,8 +464,8 @@
             wide = (wide - average) * lax.rsqrt(variance + norm_eps) * gain_all[...]
             rows_n[rows, :] = wide.astype(bf16)
 
-    def hidden_units(h, between):
-        top = pl.ds(h * expert_half, expert_half)
+    def hidden_units(b, between):
+        top = rows_of(b)
         for n in range(hid // columns):
             cols = slice(n * columns, (n + 1) * columns)
             gate = nn(rows_n[top, :], w_gate[:, cols])
@@ -447,8 +475,8 @@
 
     sib_copies, y_copies = {}, {}
 
-    def down(h, target_tp, store):
-        top = slice(h * expert_half, (h + 1) * expert_half)
+    def down(b, target_tp, store):
+        top = rows_of(b)
         for n in range(feats // out_columns):
             first = pl.multiple_of(target_tp * feats + n * out_columns, 128)
             store(
@@ -456,42 +484,46 @@
                 nn(hidden[top, :], w_down[:, pl.ds(first, out_columns)]),
             )
 
-    def give_back(h, offsets):
-        top = slice(h * expert_half, (h + 1) * expert_half)
+    def give_back(b, offsets):
         for offset in offsets:
             yt = lax.rem(my_y + offset, count_y) * CORES
 
             def to_send(rows, cols, value, offset=offset):
                 sib_send[offset, rows, cols] = value.astype(bf16)
 
-            def to_own(rows, cols, value):
-                own[rows, cols] = value
-
-            down(h, yt + 1 - my_core, to_send)
-            window = pl.ds(h * expert_half, expert_half)
-            sib_copies[h, offset] = send(
+            def to_own(rows, cols, value, offset=offset):
+                own[offset, rows, cols] = value
+
+            down(b, yt + 1 - my_core, to_send)
+            window = pl.ds(rows_of(b).start, rows_of(b).stop - rows_of(b).start)
+            sib_copies[b, offset] = send(
                 sib_send.at[offset, window], sib_recv.at[offset, window],
-                rs_s.at[offset, h], rs_r.at[offset, h], tp=sibling,
+                rs_s.at[offset, b], rs_r.at[offset, b], tp=sibling,
             )
-            down(h, yt + my_core, to_own)
-            if offset == 0:
-                continue
-            sib_copies[h, offset].wait_recv()
-            y_send[offset, top, :] = (
-                own[top, :] + sib_recv[offset, top, :].astype(f32)
+            down(b, yt + my_core, to_own)
+
+    def sum_y(b):
+        for offset in range(1, count_y):
+            sib_copies[b, offset].wait_recv()
+            rows = rows_of(b)
+            y_send[offset, rows, :] = (
+                own[offset, rows, :] + sib_recv[offset, rows, :].astype(f32)
             ).astype(bf16)
-            for g in range(h * groups_half, (h + 1) * groups_half):
-                window = pl.ds(g * group_rows, group_rows)
-                y_copies[offset, g] = send(
-                    y_send.at[offset, window], y_recv.at[offset, window],
-                    ry_s.at[offset, g], ry_r.at[offset, g], tp=yt + my_core,
-                )
+
+    def send_y(g):
+        for offset in range(1, count_y):
+            window = pl.ds(g * group_rows, group_rows)
+            y_copies[offset, g] = send(
+                y_send.at[offset, window], y_recv.at[offset, window],
+                ry_s.at[offset, g], ry_r.at[offset, g],
+                tp=lax.rem(my_y + offset, count_y) * CORES + my_core,
+            )
 
     back_copies = {}
 
     def finish(g):
         window = slice(g * group_rows, (g + 1) * group_rows)
-        total = own[window, :] + sib_recv[0, window, :].astype(f32)
+        total = own[0, window, :] + sib_recv[0, window, :].astype(f32)
         for offset in range(1, count_y):
             y_copies[offset, g].wait_recv()
             total = total + y_recv[offset, window, :].astype(f32)
@@ -510,25 +542,52 @@
             if low <= g < high:
                 copy.wait_recv()
 
-    rows_ready(0, early)
+    others = list(range(1, count_y))
+    chunks = hid // columns
+
+    def spread_out(tasks):
+        def between(n):
+            for task in tasks[n * len(tasks) // chunks : (n + 1) * len(tasks) // chunks]:
+                task()
+
+        return between
+
+    def tasks_of(function, items):
+        return [functools.partial(function, item) for item in items]
+
+    rows_ready(*blocks[0])
     for copy in gain_copies:
         copy.wait_recv()
     normalize_rows(0)
-    forward(early + 1)
     loads[14].wait()
     loads[15].wait()
-
-    def forwards(n):
-        if early + 2 + n < groups_y:
-            forward(early + 2 + n)
-
-    hidden_units(0, forwards)
-    for g in range(early + 2 + hid // columns, groups_y):
+    first = [early + 1, *range(early + 2, groups_y)]
+    after = [[] for n in range(chunks)]
+    after[max(0, chunks // 2 - 1)] += tasks_of(forward, first[:1])
+    after[max(0, chunks // 2 - 1)] += tasks_of(forward_again, [early])
+    after[-1] += tasks_of(forward, first[1:2])
+
+    def between(n):
+        for task in after[n]:
+            task()
+
+    hidden_units(0, between)
+    loads[16].wait()
+    give_back(0, others)
+    for g in first[2:]:
         forward(g)
-    forward_again(early)
+    for g in range(max(2, early - 1), early):
+        forward(g)
+    for g in range(2, early - 1):
+        forward_again(g)
+    give_back(0, [0])
     forward_again(early + 1)
-    for copy in state_copies:
-        copy.wait_recv()
+    for other, copy in state_copies:
+
+        @pl.when(other < me)
+        def _(copy=copy):
+            copy.wait_recv()
+
 
     def fold(q, carried):
         h_re, h_im = carried
@@ -579,56 +638,107 @@
     mixed_cols = pl.ds(pl.multiple_of(tp * channels, 128), channels)
     mixed_all[:, mixed_cols] = nn(order_t, mixed[...]).astype(bf16)
 
-    def mixed_window(offset):
+    piece_rows = positions // pieces
+
+    def mixed_window(offset, p):
         owner_tp = lax.rem(my_y + count_y - offset, count_y) * CORES + my_core
-        return mixed_all.at[:, pl.ds(pl.multiple_of(owner_tp * channels, 128), channels)]
-
-    mixed_y = {}
-    for k in range(1, count_y):
-        mixed_y[k] = send(
-            mixed_window(0), mixed_window(0), my_s.at[k], my_r.at[k],
-            tp=lax.rem(my_y + k, count_y) * CORES + my_core,
-        )
-    mixed_sib = [send(mixed_window(0), mixed_window(0), ms_s.at[0], ms_r.at[0], tp=sibling)]
-
-    for g in range(early + 2, groups_y):
+        return mixed_all.at[
+            pl.ds(p * piece_rows, piece_rows),
+            pl.ds(pl.multiple_of(owner_tp * channels, 128), channels),
+        ]
+
+    mixed_y, mixed_sib = {}, []
+
+    def mixed_to_sibling(offset, p):
+        here = mixed_window(offset, p)
+        mixed_sib.append(
+            (p, send(here, here, ms_s.at[offset, p], ms_r.at[offset, p], tp=sibling))
+        )
+
+    def send_mixed(p):
+        here = mixed_window(0, p)
+        for k in range(1, count_y):
+            mixed_y[k, p] = send(
+                here, here, my_s.at[k, p], my_r.at[k, p],
+                tp=lax.rem(my_y + k, count_y) * CORES + my_core,
+            )
+        mixed_to_sibling(0, p)
+
+    def forward_mixed(p):
+        for k in range(1, count_y):
+            mixed_y[k, p].wait_recv()
+            mixed_to_sibling(k, p)
+
+    send_mixed(0)
+    rows_ready(*blocks[1])
+    normalize_rows(1)
+    hidden_units(1, spread_out(tasks_of(forward_again, range(early + 2, groups_y))))
+    give_back(1, others + [0])
+    sum_y(1)
+    for g in reversed(range(*blocks[1])):
+        send_y(g)
+    for g in range(max(2, early - 1), early):
         forward_again(g)
-    rows_ready(early, groups_y)
-    normalize_rows(1)
-    hidden_units(1, lambda n: None)
-    others = list(range(1, count_y))
-    loads[16].wait()
-    give_back(1, others)
-    give_back(0, others)
-    give_back(1, [0])
+    rows_ready(*blocks[2])
+    normalize_rows(2)
+    hidden_units(2, lambda n: None)
+    give_back(2, others + [0])
+    sum_y(2)
+    for g in reversed(range(*blocks[2])):
+        send_y(g)
+    for p in range(1, pieces):
+        send_mixed(p)
+    forward_mixed(0)
+    rows_ready(*blocks[3])
     sib_copies[1, 0].wait_recv()
-    finish(groups_half)
-    give_back(0, [0])
-    for g in range(groups_half + 1, groups_half + 2):
+    sib_copies[2, 0].wait_recv()
+    for g in reversed(range(*blocks[1])):
         finish(g)
-    for k in range(1, count_y):
-        mixed_y[k].wait_recv()
-        mixed_sib.append(
-            send(mixed_window(k), mixed_window(k), ms_s.at[k], ms_r.at[k], tp=sibling)
-        )
-    for g in range(groups_half + 2, groups_y):
+    normalize_rows(3)
+    hidden_units(3, lambda n: None)
+    give_back(3, others + [0])
+    sum_y(3)
+    for g in reversed(range(*blocks[3])):
+        send_y(g)
+    sum_y(0)
+    for g in reversed(range(*blocks[0])):
+        send_y(g)
+    for g in reversed(range(*blocks[2])):
         finish(g)
     loads[8].wait()
     loads[9].wait()
-    for copy in mixed_sib:
-        copy.wait_recv()
-    out_a_cols = min(256, out_a.shape[1])
-    for n in range(out_a.shape[1] // out_a_cols):
-        cols = slice(n * out_a_cols, (n + 1) * out_a_cols)
-        value = nn(mixed_all[...], w_value[:, cols])
-        gate = nn(mixed_all[...], w_gate_out[:, cols])
-        out_a[:, cols] = (value * jax.nn.sigmoid(gate)).astype(bf16)
+
+    def project(p):
+        for copy in [copy for q, copy in mixed_sib if q == p]:
+            copy.wait_recv()
+        rows = slice(p * piece_rows, (p + 1) * piece_rows)
+        out_a_cols = min(256, out_a.shape[1])
+        for n in range(out_a.shape[1] // out_a_cols):
+            cols = slice(n * out_a_cols, (n + 1) * out_a_cols)
+            value = nn(mixed_all[rows, :], w_value[:, cols])
+            gate = nn(mixed_all[rows, :], w_gate_out[:, cols])
+            out_a[rows, cols] = (value * jax.nn.sigmoid(gate)).astype(bf16)
+
+    project(0)
+    for p in range(1, pieces):
+        forward_mixed(p)
     sib_copies[0, 0].wait_recv()
-    for g in range(groups_half):
+    sib_copies[3, 0].wait_recv()
+    for g in reversed(range(*blocks[3])):
+        finish(g)
+    for p in range(1, pieces):
+        project(p)
+    for g in reversed(range(*blocks[0])):
         finish(g)
     for k in range(1, count_ep):
         back_copies[k].wait_recv()
     out_b[...] = (tn(share_hi[...], returned[...]) + tn(share_lo[...], returned[...])).astype(bf16)
+    for other, copy in state_copies:
+
+        @pl.when(other > me)
+        def _(copy=copy):
+            copy.wait_send()
+
     for copy in pending:
         copy.wait_send()
 
@@ -643,7 +753,7 @@
     slots = count_ep * capacity
     hid = args[14].shape[1]
     width = feats * count_tp
-    groups_y, halves = min(count_ep, 8), 2
+    groups_y, pieces = min(count_ep, 8), 2
     dma = pltpu.SemaphoreType.DMA
     vmem = pltpu.VMEM
     scratch = [vmem(x.shape, x.dtype) for x in args] + [
@@ -671,7 +781,7 @@
         vmem((positions, channels), bf16),
         vmem((positions, channels * count_tp), bf16),
         vmem((slots, hid), bf16),
-        vmem((slots, feats), f32),
+        vmem((count_y, slots, feats), f32),
         vmem((count_y, slots, feats), bf16),
         vmem((count_y, slots, feats), bf16),
         vmem((count_y, slots, feats), bf16),
@@ -679,21 +789,21 @@
         vmem((slots, feats), bf16),
         vmem((slots, feats), bf16),
         dma((len(args),)),
-        dma((2,)), dma((2,)),
+        dma((3,)), dma((3,)),
         dma((count_tp,)), dma((count_tp,)),
         dma((count_tp,)), dma((count_tp,)),
-        dma((count_ep,)), dma((count_ep,)),
+        dma((2, count_ep)), dma((2, count_ep)),
         dma((count_y, groups_y)), dma((count_y, groups_y)),
         dma((count_y, groups_y)), dma((count_y, groups_y)),
         dma((count_ep,)), dma((count_ep,)),
-        dma((count_y,)), dma((count_y,)),
-        dma((count_y,)), dma((count_y,)),
-        dma((count_y, halves)), dma((count_y, halves)),
+        dma((count_y, pieces)), dma((count_y, pieces)),
+        dma((count_y, pieces)), dma((count_y, pieces)),
+        dma((count_y, 4)), dma((count_y, 4)),
         dma((count_y, groups_y)), dma((count_y, groups_y)),
         dma((count_ep,)), dma((count_ep,)),
     ]
     return pl.pallas_call(
-        functools.partial(kernel, (count_ep, count_tp, groups_y, halves, state_size)),
+        functools.partial(kernel, (count_ep, count_tp, groups_y, pieces, state_size)),
         out_shape=[
             vmem((positions, args[8].shape[1]), bf16),
             vmem((tokens, feats), bf16),

time: 53 us -> 49.4 us (0.932)
  Pallas kernels: 50.8 us -> 47.3 us
    pallas_call x1, Pallas kernels: 50.8 us -> 47.3 us  [fused(): pl.pallas_call(functools.partial(kernel, (count_ep, count_tp, groups_y, p...]
where the time goes in v3:
time: 49.4 us; the launch traced here: 49.3 us
  Pallas kernels  47.3 us (96%)
  local copies, waits for them, and re-layouts  1.36 us (3%)
  between operations  0.65 us (1%)
    pallas_call x1, Pallas kernels, fused(): pl.pallas_call(functools.partial(kernel, (count_ep, count_tp, groups_y, p...  47.3 us
    unnamed x2, local copies, waits for them, and re-layouts  1.36 us

profile of v3, /device:TPU:0, one launch (start us, length us, event | category | flops | bytes accessed | tf_op | source)
XLA Modules:
  0.0 49.3 jit_solution(5068333791262105415)
XLA Ops:
  0.6 47.3 %shard_map.185 = (bf16[256,512]{1,0:T(8,128)(2,1)S(1)}, bf16[128,512]{1,0:T(8,128)(2,1)S(1)}) custom-call(bf16[256,512]{1,0:T(8,128)(2,1)} %refs_0_.1, f32[32,256]{1,0:T(8,128)} %bitcast.23, f32[1,512]{1,0:T(1,128)} %bitcast.24, f32[32,32]{1,0:T(8,128)} %refs_3_.1, f32[512,32]{1,0:T(8,128)} %bitcast.19, f32[512,32]{1,0:T(8,128)} %bitcast.20, ...), custom_call_target="tpu_custom_call" | custom-call | tf_op jit(solution)/shard_map/pallas_call | solution.py:805
  47.9 0.7 %copy.22 = bf16[256,512]{1,0:T(8,128)(2,1)} copy(bf16[256,512]{1,0:T(8,128)(2,1)S(1)} %get-tuple-element.2) | data formatting | bytes 524288
  48.6 0.7 %copy.23 = bf16[128,512]{1,0:T(8,128)(2,1)} copy(bf16[128,512]{1,0:T(8,128)(2,1)S(1)} %get-tuple-element.3) | data formatting | bytes 262144

commit v4 on v3

--- a/solution.py
+++ b/solution.py
@@ -93,8 +93,7 @@
         mine_stats, slot_stats, pole, tokens_far, routes_far, gain_all, rows_n, outgoing, rows_x, share_hi, share_lo, a_re, a_im, u_re, u_im,
         sums, enter, mine_state, slot_state, n_re, n_im, mixed, mixed_all, hidden, own,
         sib_send, sib_recv, y_send, y_recv, final, returned,
-        sem_in, far_s, far_r, gn_s, gn_r, st_s, st_r, aa_s, aa_r, dy_s, dy_r, ds_s, ds_r, hs_s, hs_r,
-        my_s, my_r, ms_s, ms_r, rs_s, rs_r, ry_s, ry_r, ra_s, ra_r,
+        sem_in, sem_far, sem_small, sem_send, aa_r, dy_r, ds_r, hs_s, hs_r, my_r, ms_r, rs_r, ry_r,
     ) = refs
     (
         a_in, step_in, gain_a, real_in, in_re, in_im, rd_re, rd_im, w_value, w_gate_out,
@@ -126,16 +125,16 @@
     for i in (10, 12, 11, 0, 1, 3, 17, 2, 13, 4, 5, 6, 7, 14, 15, 16, 8, 9):
         loads[i].start()
 
-    pending = []
-
     def send(source, target, send_sem, recv_sem, **where):
         copy = pltpu.make_async_remote_copy(
             src_ref=source, dst_ref=target, send_sem=send_sem, recv_sem=recv_sem,
             device_id=where, device_id_type=pl.DeviceIdType.MESH,
         )
         copy.start()
-        pending.append(copy)
         return copy
+
+    def drain(sem, ref):
+        pltpu.make_async_copy(ref, ref, sem).wait()
 
     positions, channels = a_in.shape
     tokens, feats = b_in.shape
@@ -157,19 +156,19 @@
     for i in (12, 11, 10):
         loads[i].wait()
     pl.semaphore_wait(barrier, count_ep + count_tp - 2)
-    far_routes = send(routes_in, routes_far, far_s.at[0], far_r.at[0], ep=portal)
+    far_routes = send(routes_in, routes_far, sem_far.at[0], sem_far.at[1], ep=portal)
     cuts = 2 if feats % 256 == 0 else 1
     cut = [slice(c * feats // cuts, (c + 1) * feats // cuts) for c in range(cuts)]
     far_tokens = [
         send(
-            b_in.at[:, cut[c]], tokens_far.at[:, cut[c]], far_s.at[1 + c], far_r.at[1 + c],
+            b_in.at[:, cut[c]], tokens_far.at[:, cut[c]], sem_far.at[2], sem_far.at[3 + c],
             ep=portal,
         )
         for c in range(cuts)
     ]
     gain_copies = [
         send(
-            gain_b, gain_all.at[:, my_cols], gn_s.at[k], gn_r.at[k], tp=lax.rem(tp + k, count_tp)
+            gain_b, gain_all.at[:, my_cols], sem_small.at[0], sem_small.at[1], tp=lax.rem(tp + k, count_tp)
         )
         for k in range(1, count_tp)
     ]
@@ -202,7 +201,7 @@
     chosen_near = select(owner_near, place_own)
     chosen = chosen_near.astype(f32).astype(bf16)
 
-    arrivals = {}
+    arrivals = set()
 
     def hand_out(base, columns, values, c):
         outgoing[base * cap : (base + near) * cap, columns] = values
@@ -210,17 +209,17 @@
         there = pl.ds(pl.multiple_of(tp * feats + columns.start, 128), size)
         for k in range(1, near):
             here = pl.ds((base + k) * cap, cap)
-            arrivals.setdefault(base + k, []).append(
-                send(
-                    outgoing.at[here, columns], rows_x.at[here, there], aa_s.at[c, base + k],
-                    aa_r.at[c, base + k], ep=partner(me, k),
-                )
+            arrivals.add(base + k)
+            send(
+                outgoing.at[here, columns], rows_x.at[here, there], sem_send.at[0],
+                aa_r.at[base + k], ep=partner(me, k),
             )
         rows_x[base * cap : (base + 1) * cap, there] = values[0:cap]
 
     per_group = count_ep // groups_y
     group_rows = per_group * cap
-    y_arrivals, sib_arrivals = {}, []
+    y_arrivals = {}
+    block_of = [g // (groups_y // 4) if groups_y >= 4 else g for g in range(groups_y)]
 
     def core_cols(offset):
         owner_tp = lax.rem(my_y + count_y - offset, count_y) * CORES + my_core
@@ -228,16 +227,16 @@
 
     def to_sibling(offset, g):
         here = rows_x.at[pl.ds(g * group_rows, group_rows), core_cols(offset)]
-        sib_arrivals.append((g, send(here, here, ds_s.at[offset, g], ds_r.at[offset, g], tp=sibling)))
+        send(here, here, sem_send.at[1], ds_r.at[block_of[g]], tp=sibling)
 
     def forward(g):
         for k in range(g * per_group, (g + 1) * per_group):
-            for copy in arrivals.get(k, []):
-                copy.wait_recv()
+            if k in arrivals:
+                drain(aa_r.at[k], final.at[pl.ds(0, cap)])
         here = rows_x.at[pl.ds(g * group_rows, group_rows), my_cols]
         for k in range(1, count_y):
             y_arrivals[k, g] = send(
-                here, here, dy_s.at[k, g], dy_r.at[k, g],
+                here, here, sem_send.at[2], dy_r.at[k - 1, g],
                 tp=lax.rem(my_y + k, count_y) * CORES + my_core,
             )
         to_sibling(0, g)
@@ -252,7 +251,7 @@
     loads[0].wait()
     mine_stats[...] = row_sums(a_in[...])
     stat_copies = [
-        send(mine_stats, slot_stats.at[k], st_s.at[k], st_r.at[k], tp=lax.rem(tp + k, count_tp))
+        send(mine_stats, slot_stats.at[k], sem_small.at[2], sem_small.at[3], tp=lax.rem(tp + k, count_tp))
         for k in range(1, count_tp)
     ]
 
@@ -350,8 +349,7 @@
 
     for c in range(cuts - 1):
         hand_out_far(c)
-    for copy in stat_copies:
-        copy.wait_recv()
+    drain(sem_small.at[3], slot_stats.at[pl.ds(1, count_tp - 1)])
     total = mine_stats[...]
     for k in range(1, count_tp):
         total = total + slot_stats[k]
@@ -498,7 +496,7 @@
             window = pl.ds(rows_of(b).start, rows_of(b).stop - rows_of(b).start)
             sib_copies[b, offset] = send(
                 sib_send.at[offset, window], sib_recv.at[offset, window],
-                rs_s.at[offset, b], rs_r.at[offset, b], tp=sibling,
+                sem_send.at[3], rs_r.at[offset, b], tp=sibling,
             )
             down(b, yt + my_core, to_own)
 
@@ -515,7 +513,7 @@
             window = pl.ds(g * group_rows, group_rows)
             y_copies[offset, g] = send(
                 y_send.at[offset, window], y_recv.at[offset, window],
-                ry_s.at[offset, g], ry_r.at[offset, g],
+                sem_send.at[4], ry_r.at[offset - 1, g],
                 tp=lax.rem(my_y + offset, count_y) * CORES + my_core,
             )
 
@@ -534,13 +532,18 @@
         for k in range(max(1, g * per_group), (g + 1) * per_group):
             here = pl.ds(k * cap, cap)
             back_copies[k] = send(
-                final.at[here], returned.at[here], ra_s.at[k], ra_r.at[k], ep=partner(me, k)
+                final.at[here], returned.at[here], sem_send.at[5], sem_small.at[4], ep=partner(me, k)
             )
 
     def rows_ready(low, high):
-        for g, copy in list(sib_arrivals):
-            if low <= g < high:
-                copy.wait_recv()
+        size = (high - low) * group_rows
+        drain_rows(ds_r.at[block_of[low]], count_y * size)
+
+    def drain_rows(sem, count):
+        if count <= slots:
+            drain(sem, final.at[pl.ds(0, count)])
+        else:
+            drain(sem, rows_x.at[:, pl.ds(0, count // slots * feats)])
 
     others = list(range(1, count_y))
     chunks = hid // columns
@@ -556,8 +559,7 @@
         return [functools.partial(function, item) for item in items]
 
     rows_ready(*blocks[0])
-    for copy in gain_copies:
-        copy.wait_recv()
+    drain(sem_small.at[1], gain_all.at[:, pl.ds(0, width - feats)])
     normalize_rows(0)
     loads[14].wait()
     loads[15].wait()
@@ -647,19 +649,17 @@
             pl.ds(pl.multiple_of(owner_tp * channels, 128), channels),
         ]
 
-    mixed_y, mixed_sib = {}, []
+    mixed_y = {}
 
     def mixed_to_sibling(offset, p):
         here = mixed_window(offset, p)
-        mixed_sib.append(
-            (p, send(here, here, ms_s.at[offset, p], ms_r.at[offset, p], tp=sibling))
-        )
+        send(here, here, sem_send.at[6], ms_r.at[p], tp=sibling)
 
     def send_mixed(p):
         here = mixed_window(0, p)
         for k in range(1, count_y):
             mixed_y[k, p] = send(
-                here, here, my_s.at[k, p], my_r.at[k, p],
+                here, here, sem_send.at[7], my_r.at[k - 1, p],
                 tp=lax.rem(my_y + k, count_y) * CORES + my_core,
             )
         mixed_to_sibling(0, p)
@@ -709,8 +709,7 @@
     loads[9].wait()
 
     def project(p):
-        for copy in [copy for q, copy in mixed_sib if q == p]:
-            copy.wait_recv()
+        drain(ms_r.at[p], mixed_all.at[pl.ds(0, piece_rows), pl.ds(0, count_y * channels)])
         rows = slice(p * piece_rows, (p + 1) * piece_rows)
         out_a_cols = min(256, out_a.shape[1])
         for n in range(out_a.shape[1] // out_a_cols):
@@ -730,8 +729,7 @@
         project(p)
     for g in reversed(range(*blocks[0])):
         finish(g)
-    for k in range(1, count_ep):
-        back_copies[k].wait_recv()
+    drain(sem_small.at[4], returned.at[pl.ds(cap, slots - cap)])
     out_b[...] = (tn(share_hi[...], returned[...]) + tn(share_lo[...], returned[...])).astype(bf16)
     for other, copy in state_copies:
 
@@ -739,8 +737,18 @@
         def _(copy=copy):
             copy.wait_send()
 
-    for copy in pending:
-        copy.wait_send()
+    far_routes.wait_send()
+    drain(sem_far.at[2], tokens_far)
+    drain(sem_small.at[0], gain_all.at[:, pl.ds(0, width - feats)])
+    drain(sem_small.at[2], slot_stats.at[pl.ds(1, count_tp - 1)])
+    drain_rows(sem_send.at[0], 2 * (near - 1) * cap)
+    drain_rows(sem_send.at[1], count_y * slots)
+    drain_rows(sem_send.at[2], (count_y - 1) * slots)
+    drain_rows(sem_send.at[3], count_y * slots)
+    drain_rows(sem_send.at[4], (count_y - 1) * slots)
+    drain_rows(sem_send.at[5], slots - cap)
+    drain(sem_send.at[6], mixed_all.at[:, pl.ds(0, count_y * channels)])
+    drain(sem_send.at[7], mixed_all.at[:, pl.ds(0, (count_y - 1) * channels)])
 
 
 def fused(args, state_size, capacity):
@@ -789,18 +797,17 @@
         vmem((slots, feats), bf16),
         vmem((slots, feats), bf16),
         dma((len(args),)),
-        dma((3,)), dma((3,)),
-        dma((count_tp,)), dma((count_tp,)),
-        dma((count_tp,)), dma((count_tp,)),
-        dma((2, count_ep)), dma((2, count_ep)),
-        dma((count_y, groups_y)), dma((count_y, groups_y)),
-        dma((count_y, groups_y)), dma((count_y, groups_y)),
+        dma((5,)),
+        dma((5,)),
+        dma((8,)),
+        dma((count_ep,)),
+        dma((count_y - 1, groups_y)),
+        dma((4,)),
         dma((count_ep,)), dma((count_ep,)),
-        dma((count_y, pieces)), dma((count_y, pieces)),
-        dma((count_y, pieces)), dma((count_y, pieces)),
-        dma((count_y, 4)), dma((count_y, 4)),
-        dma((count_y, groups_y)), dma((count_y, groups_y)),
-        dma((count_ep,)), dma((count_ep,)),
+        dma((count_y - 1, pieces)),
+        dma((pieces,)),
+        dma((count_y, 4)),
+        dma((count_y - 1, groups_y)),
     ]
     return pl.pallas_call(
         functools.partial(kernel, (count_ep, count_tp, groups_y, pieces, state_size)),
@@ -817,6 +824,17 @@
     )(*args)
 
 
+def write_out(a_ref, b_ref, a_out, b_out, sems):
+    copies = [
+        pltpu.make_async_copy(source, target, sems.at[i])
+        for i, (source, target) in enumerate(((a_ref, a_out), (b_ref, b_out)))
+    ]
+    for copy in copies:
+        copy.start()
+    for copy in copies:
+        copy.wait()
+
+
 def shards(
     mixer_input, mixer_gain, time_step, pole_real, pole_imag, input_real, input_imag,
     read_real, read_imag, out_value, out_gate, expert_input, expert_gain, routes,
@@ -834,7 +852,17 @@
         out_value, out_gate, expert_input, expert_gain[None, :], routes.T, route_weight.T,
         expert_gate[0], expert_up[0], expert_down[0], pole_imag,
     )
-    return tuple(fused(args, pole_real.shape[1], capacity))
+    results = fused(args, pole_real.shape[1], capacity)
+    return tuple(
+        pl.pallas_call(
+            write_out,
+            out_shape=[jax.ShapeDtypeStruct(x.shape, x.dtype) for x in results],
+            in_specs=[pl.BlockSpec(memory_space=pltpu.VMEM)] * 2,
+            out_specs=[pl.BlockSpec(memory_space=pltpu.HBM)] * 2,
+            scratch_shapes=[pltpu.SemaphoreType.DMA((2,))],
+            compiler_params=pltpu.CompilerParams(vmem_limit_bytes=1024 * 1024),
+        )(*results)
+    )
 
 
 def solution(mesh):

time: 49.4 us -> 47.6 us (0.964)
  local copies, waits for them, and re-layouts: 1.36 us -> 0 us
  Pallas kernels: 47.3 us -> 46.7 us
    unnamed x2 -> x0, local copies, waits for them, and re-layouts: 1.36 us -> none
    pallas_call x1, Pallas kernels: 47.3 us -> 45.9 us  [fused(): pl.pallas_call(functools.partial(kernel, (count_ep, count_tp, groups_y, p...]
    pallas_call x0 -> x1, Pallas kernels: none -> 0.76 us  [shards(): pl.pallas_call(write_out, out_shape=[jax.ShapeDtypeStruct(x.shape, x.dtyp...]
where the time goes in v4:
time: 47.6 us; the launch traced here: 47.5 us
  Pallas kernels  46.7 us (98%)
  between operations  0.81 us (2%)
    pallas_call x1, Pallas kernels, fused(): pl.pallas_call(functools.partial(kernel, (count_ep, count_tp, groups_y, p...  45.9 us

profile of v4, /device:TPU:0, one launch (start us, length us, event | category | flops | bytes accessed | tf_op | source)
XLA Modules:
  0.0 47.5 jit_solution(13804587234616190002)
XLA Ops:
  0.6 45.9 %shard_map.185 = (bf16[256,512]{1,0:T(8,128)(2,1)S(1)}, bf16[128,512]{1,0:T(8,128)(2,1)S(1)}) custom-call(bf16[256,512]{1,0:T(8,128)(2,1)} %refs_0_.1, f32[32,256]{1,0:T(8,128)} %bitcast.23, f32[1,512]{1,0:T(1,128)} %bitcast.24, f32[32,32]{1,0:T(8,128)} %refs_3_.1, f32[512,32]{1,0:T(8,128)} %bitcast.19, f32[512,32]{1,0:T(8,128)} %bitcast.20, ...), custom_call_target="tpu_custom_call" | custom-call | tf_op jit(solution)/shard_map/pallas_call | solution.py:812
  46.6 0.8 %shard_map.186 = (bf16[256,512]{1,0:T(8,128)(2,1)}, bf16[128,512]{1,0:T(8,128)(2,1)}) custom-call(bf16[256,512]{1,0:T(8,128)(2,1)S(1)} %get-tuple-element.4.a_ref, bf16[128,512]{1,0:T(8,128)(2,1)S(1)} %get-tuple-element.5.b_ref), custom_call_target="tpu_custom_call" | custom-call | tf_op jit(solution)/shard_map/pallas_call | solution.py:857

commit v5 on v4

--- a/solution.py
+++ b/solution.py
@@ -203,18 +203,23 @@
 
     arrivals = set()
 
-    def hand_out(base, columns, values, c):
+    def hand_out(base, columns, values, ks):
         outgoing[base * cap : (base + near) * cap, columns] = values
+        rows_x[base * cap : (base + 1) * cap, window_of(columns)] = values[0:cap]
+        send_slabs(base, columns, ks)
+
+    def window_of(columns):
         size = columns.stop - columns.start
-        there = pl.ds(pl.multiple_of(tp * feats + columns.start, 128), size)
-        for k in range(1, near):
+        return pl.ds(pl.multiple_of(tp * feats + columns.start, 128), size)
+
+    def send_slabs(base, columns, ks):
+        for k in ks:
             here = pl.ds((base + k) * cap, cap)
             arrivals.add(base + k)
             send(
-                outgoing.at[here, columns], rows_x.at[here, there], sem_send.at[0],
+                outgoing.at[here, columns], rows_x.at[here, window_of(columns)], sem_send.at[0],
                 aa_r.at[base + k], ep=partner(me, k),
             )
-        rows_x[base * cap : (base + 1) * cap, there] = values[0:cap]
 
     per_group = count_ep // groups_y
     group_rows = per_group * cap
@@ -246,7 +251,8 @@
             y_arrivals[k, g].wait_recv()
             to_sibling(k, g)
 
-    hand_out(0, slice(0, feats), nn(chosen, b_in[...]).astype(bf16), 0)
+    near_first = max(2, near // 2)
+    hand_out(0, slice(0, feats), nn(chosen, b_in[...]).astype(bf16), range(1, near))
     forward(0)
     loads[0].wait()
     mine_stats[...] = row_sums(a_in[...])
@@ -345,7 +351,7 @@
 
     def hand_out_far(c):
         far_tokens[c].wait_recv()
-        hand_out(near, cut[c], nn(chosen_far, tokens_far[:, cut[c]]).astype(bf16), c)
+        hand_out(near, cut[c], nn(chosen_far, tokens_far[:, cut[c]]).astype(bf16), range(1, near))
 
     for c in range(cuts - 1):
         hand_out_far(c)
@@ -389,7 +395,11 @@
         sums[2, :, lanes], sums[3, :, lanes] = lax.fori_loop(0, steps, one, (zero, zero), unroll=2)
 
     early = groups_y // 2
-    for t in range(tiles):
+    for t in range(tiles // 2):
+        first_half(t)
+    hand_out_far(cuts - 1)
+    forward(early)
+    for t in range(tiles // 2, tiles):
         first_half(t)
     for base in range(0, flat, span):
         chunk_sums(base)
@@ -421,9 +431,7 @@
         def _(copy=copy):
             copy.start()
 
-    hand_out_far(cuts - 1)
-    forward(early)
-    for g in range(2, early - 1):
+    for g in range(2, min(3, early)):
         forward(g)
     forward_again(1)
     loads[13].wait()
@@ -578,10 +586,6 @@
     give_back(0, others)
     for g in first[2:]:
         forward(g)
-    for g in range(max(2, early - 1), early):
-        forward(g)
-    for g in range(2, early - 1):
-        forward_again(g)
     give_back(0, [0])
     forward_again(early + 1)
     for other, copy in state_copies:
@@ -630,6 +634,8 @@
             return s_re, s_im
 
         lax.fori_loop(0, steps // 2, advance, (enter[0, :, lanes], enter[1, :, lanes]))
+    for g in range(3, early):
+        forward(g)
     for t in range(tiles):
         lanes = slice(t * tile, (t + 1) * tile)
         table = slice(t * tile_ch, (t + 1) * tile_ch)
@@ -677,33 +683,37 @@
     sum_y(1)
     for g in reversed(range(*blocks[1])):
         send_y(g)
-    for g in range(max(2, early - 1), early):
-        forward_again(g)
     rows_ready(*blocks[2])
     normalize_rows(2)
-    hidden_units(2, lambda n: None)
+    hidden_units(2, spread_out(tasks_of(forward_again, range(2, early))))
     give_back(2, others + [0])
     sum_y(2)
     for g in reversed(range(*blocks[2])):
         send_y(g)
-    for p in range(1, pieces):
-        send_mixed(p)
+    sum_y(0)
+    for g in reversed(range(1, split)):
+        send_y(g)
     forward_mixed(0)
     rows_ready(*blocks[3])
+    normalize_rows(3)
     sib_copies[1, 0].wait_recv()
     sib_copies[2, 0].wait_recv()
-    for g in reversed(range(*blocks[1])):
-        finish(g)
-    normalize_rows(3)
-    hidden_units(3, lambda n: None)
+    far_order = list(reversed(range(*blocks[1]))) + list(reversed(range(*blocks[2])))
+
+    def one_finish(n):
+        if n == chunks - 1:
+            finish(far_order[0])
+            finish(far_order[1])
+
+    hidden_units(3, one_finish)
     give_back(3, others + [0])
     sum_y(3)
     for g in reversed(range(*blocks[3])):
         send_y(g)
-    sum_y(0)
-    for g in reversed(range(*blocks[0])):
-        send_y(g)
-    for g in reversed(range(*blocks[2])):
+    for p in range(1, pieces):
+        send_mixed(p)
+    send_y(0)
+    for g in far_order[2:]:
         finish(g)
     loads[8].wait()
     loads[9].wait()
@@ -719,16 +729,17 @@
             out_a[rows, cols] = (value * jax.nn.sigmoid(gate)).astype(bf16)
 
     project(0)
-    for p in range(1, pieces):
-        forward_mixed(p)
     sib_copies[0, 0].wait_recv()
     sib_copies[3, 0].wait_recv()
+    for g in reversed(range(1, split)):
+        finish(g)
     for g in reversed(range(*blocks[3])):
         finish(g)
     for p in range(1, pieces):
+        forward_mixed(p)
+    finish(0)
+    for p in range(1, pieces):
         project(p)
-    for g in reversed(range(*blocks[0])):
-        finish(g)
     drain(sem_small.at[4], returned.at[pl.ds(cap, slots - cap)])
     out_b[...] = (tn(share_hi[...], returned[...]) + tn(share_lo[...], returned[...])).astype(bf16)
     for other, copy in state_copies:

time: 47.6 us -> 45.7 us (0.960)
  Pallas kernels: 46.7 us -> 44.7 us
    pallas_call x1, Pallas kernels: 45.9 us -> 44 us  [fused(): pl.pallas_call(functools.partial(kernel, (count_ep, count_tp, groups_y, p...]
where the time goes in v5:
time: 45.7 us; the launch traced here: 45.5 us
  Pallas kernels  44.7 us (98%)
  between operations  0.81 us (2%)
    pallas_call x1, Pallas kernels, fused(): pl.pallas_call(functools.partial(kernel, (count_ep, count_tp, groups_y, p...  44 us

profile of v5, /device:TPU:0, one launch (start us, length us, event | category | flops | bytes accessed | tf_op | source)
XLA Modules:
  0.0 45.5 jit_solution(10502852235379095903)
XLA Ops:
  0.6 44.0 %shard_map.185 = (bf16[256,512]{1,0:T(8,128)(2,1)S(1)}, bf16[128,512]{1,0:T(8,128)(2,1)S(1)}) custom-call(bf16[256,512]{1,0:T(8,128)(2,1)} %refs_0_.1, f32[32,256]{1,0:T(8,128)} %bitcast.23, f32[1,512]{1,0:T(1,128)} %bitcast.24, f32[32,32]{1,0:T(8,128)} %refs_3_.1, f32[512,32]{1,0:T(8,128)} %bitcast.19, f32[512,32]{1,0:T(8,128)} %bitcast.20, ...), custom_call_target="tpu_custom_call" | custom-call | tf_op jit(solution)/shard_map/pallas_call | solution.py:823
  44.6 0.8 %shard_map.186 = (bf16[256,512]{1,0:T(8,128)(2,1)}, bf16[128,512]{1,0:T(8,128)(2,1)}) custom-call(bf16[256,512]{1,0:T(8,128)(2,1)S(1)} %get-tuple-element.4.a_ref, bf16[128,512]{1,0:T(8,128)(2,1)S(1)} %get-tuple-element.5.b_ref), custom_call_target="tpu_custom_call" | custom-call | tf_op jit(solution)/shard_map/pallas_call | solution.py:868

commit v6 on v5

--- a/solution.py
+++ b/solution.py
@@ -395,10 +395,10 @@
         sums[2, :, lanes], sums[3, :, lanes] = lax.fori_loop(0, steps, one, (zero, zero), unroll=2)
 
     early = groups_y // 2
+    hand_out_far(cuts - 1)
+    forward(early)
     for t in range(tiles // 2):
         first_half(t)
-    hand_out_far(cuts - 1)
-    forward(early)
     for t in range(tiles // 2, tiles):
         first_half(t)
     for base in range(0, flat, span):
@@ -566,6 +566,7 @@
     def tasks_of(function, items):
         return [functools.partial(function, item) for item in items]
 
+    forward(early + 1)
     rows_ready(*blocks[0])
     drain(sem_small.at[1], gain_all.at[:, pl.ds(0, width - feats)])
     normalize_rows(0)
@@ -573,9 +574,9 @@
     loads[15].wait()
     first = [early + 1, *range(early + 2, groups_y)]
     after = [[] for n in range(chunks)]
-    after[max(0, chunks // 2 - 1)] += tasks_of(forward, first[:1])
-    after[max(0, chunks // 2 - 1)] += tasks_of(forward_again, [early])
-    after[-1] += tasks_of(forward, first[1:2])
+    after[0] += tasks_of(forward_again, [early])
+    after[max(0, chunks // 2 - 1)] += tasks_of(forward, first[1:2])
+    after[-1] += tasks_of(forward, first[2:3])
 
     def between(n):
         for task in after[n]:
@@ -584,7 +585,7 @@
     hidden_units(0, between)
     loads[16].wait()
     give_back(0, others)
-    for g in first[2:]:
+    for g in first[3:]:
         forward(g)
     give_back(0, [0])
     forward_again(early + 1)

time: 45.7 us -> 45.6 us (level)
  no operation moved by 1% of the time
where the time goes in v6:
time: 45.6 us; the launch traced here: 45.4 us
  Pallas kernels  44.6 us (98%)
  between operations  0.81 us (2%)
    pallas_call x1, Pallas kernels, fused(): pl.pallas_call(functools.partial(kernel, (count_ep, count_tp, groups_y, p...  43.9 us

profile of v6, /device:TPU:0, one launch (start us, length us, event | category | flops | bytes accessed | tf_op | source)
XLA Modules:
  0.0 45.4 jit_solution(17308283479662250364)
XLA Ops:
  0.6 43.9 %shard_map.185 = (bf16[256,512]{1,0:T(8,128)(2,1)S(1)}, bf16[128,512]{1,0:T(8,128)(2,1)S(1)}) custom-call(bf16[256,512]{1,0:T(8,128)(2,1)} %refs_0_.1, f32[32,256]{1,0:T(8,128)} %bitcast.23, f32[1,512]{1,0:T(1,128)} %bitcast.24, f32[32,32]{1,0:T(8,128)} %refs_3_.1, f32[512,32]{1,0:T(8,128)} %bitcast.19, f32[512,32]{1,0:T(8,128)} %bitcast.20, ...), custom_call_target="tpu_custom_call" | custom-call | tf_op jit(solution)/shard_map/pallas_call | solution.py:824
  44.5 0.8 %shard_map.186 = (bf16[256,512]{1,0:T(8,128)(2,1)}, bf16[128,512]{1,0:T(8,128)(2,1)}) custom-call(bf16[256,512]{1,0:T(8,128)(2,1)S(1)} %get-tuple-element.4.a_ref, bf16[128,512]{1,0:T(8,128)(2,1)S(1)} %get-tuple-element.5.b_ref), custom_call_target="tpu_custom_call" | custom-call | tf_op jit(solution)/shard_map/pallas_call | solution.py:869
